TPU v7x, 32 devices: a whole 2x2x4 slice. The times are simulated.
32 devices in a mesh: grp: 2 (over y), sp: 4 (over z), tp: 2 (over x), dp: 2 (over core).
Axes of the slice: x: 2, y: 2, z: 4, core: 2. Of those that a mesh axis runs over, the one named last changes fastest.
Arguments:
- latent: bfloat16 [6144, 4096], P(('grp', 'sp', 'dp')), parts along dimension 0, may hold values from -6 to 6
- context: bfloat16 [1024, 4096], P(('grp', 'sp')), parts along dimension 0, may hold values from -6 to 6
- condition: bfloat16 [8192], P('grp'), parts along dimension 0, may hold values from -6 to 6
- context_condition: bfloat16 [4096], replicated, may hold values from -6 to 6
- shift_weight: bfloat16 [4096, 4096], P('sp', ('tp', 'dp')), may hold values from -0.09375 to 0.09375
- scale_weight: bfloat16 [4096, 4096], P('sp', ('tp', 'dp')), may hold values from -0.09375 to 0.09375
- gate_weight: bfloat16 [4096, 4096], P('sp', ('tp', 'dp')), may hold values from -0.09375 to 0.09375
- norm_gain: float32 [4096], replicated, may hold values from 0.1 to 1.9
- out_gate_weight: bfloat16 [4096, 2048], P(None, ('tp', 'dp')), may hold values from -0.09375 to 0.09375
- signal_weight: bfloat16 [4096, 2048], P(None, ('tp', 'dp')), may hold values from -0.09375 to 0.09375
- writer_weight: bfloat16 [4096, 1024], P(None, ('tp', 'dp')), may hold values from -0.09375 to 0.09375
- reader_matrix: bfloat16 [4096, 1024], P(None, ('tp', 'dp')), may hold values from -0.09375 to 0.09375
- step_weight: bfloat16 [2, 4096, 32], P(None, None, ('tp', 'dp')), may hold values from -0.09375 to 0.09375
- signal_taps: float32 [3, 2048], P(None, ('tp', 'dp')), may hold values from -3.5 to 3.5
- writer_taps: float32 [3, 1024], P(None, ('tp', 'dp')), may hold values from -3.5 to 3.5
- reader_taps: float32 [3, 1024], P(None, ('tp', 'dp')), may hold values from -3.5 to 3.5
- step_bias: float32 [2, 32], P(None, ('tp', 'dp')), may hold values from -4.5 to -2.5
- decay_log: float32 [2, 32], P(None, ('tp', 'dp')), may hold values from -12 to 1
- decay_extra: float32 [2, 32, 6144], P(None, ('tp', 'dp'), ('grp', 'sp')), parts along dimension 2, may hold values from -3 to 0
- group_gain: float32 [2048], P(('tp', 'dp')), may hold values from 0.1 to 1.9
- output_weight: bfloat16 [2048, 4096], P(None, ('tp', 'dp')), may hold values from -0.125 to 0.125
Outputs:
- updated: bfloat16 [6144, 4096], P(('grp', 'sp'), ('tp', 'dp')), parts along dimension 0
There are 2 independent parts, one for each index of `grp`. A program takes and returns all parts, laid end to end along the dimension named above; an argument that names none is the same for every part. Nothing has to cross between parts.
All inputs are finite; a program needn't handle non-finite values.
Results may differ from a plain program's by a relative error of at most 0.007.
Values may be sent and summed in bfloat16 or wider, within the bound.
A program may use at most 128 MiB of HBM per device.

v0:
```python
import functools

import jax
import jax.numpy as jnp
from jax import lax
from jax.experimental import pallas as pl
from jax.experimental.pallas import tpu as pltpu
from jax.sharding import PartitionSpec as P

STATE = 128
BLOCK = 128
EPSILON = 1e-06
TILE_N = 256
F32 = jnp.float32
BF16 = jnp.bfloat16
MESH = pl.DeviceIdType.MESH


def silu(v):
    return v / (1.0 + jnp.exp(-v))


def softplus(v):
    return jnp.maximum(v, 0.0) + jnp.log1p(jnp.exp(-jnp.abs(v)))


def dot(a, b):
    return jnp.dot(a, b, preferred_element_type=F32)


def thirds(v):
    first = v.astype(BF16)
    rest = v - first.astype(F32)
    second = rest.astype(BF16)
    third = (rest - second.astype(F32)).astype(BF16)
    return first, second, third


def kernel(dims, *refs):
    (
        latent, context, cond, ctx_cond, shift_w, scale_w, gate_w, gain,
        w_gate, w_sig, w_wr, w_rd, w_step, taps, step_bias, decay_log, extra,
        group_gain, w_out, out,
        lat_v, ctx_v, act, mod_w, mod_part, gate_part, mod_in, gate_in, mod_sum, mod_all,
        scale_rows, shift_rows, edge_out, edge_in, edge_rows, hid, hid_c, w_all, w_st, w_o,
        raw, raw_c, st_raw, cum_col, ecum_col, cum_row, step_row, sig, wr, rd,
        states, dec, ent, ctx_acc, ctx_dec, ctx_send, ctx_recv, cdec_send, cdec_recv,
        span_total, chain_out, chain_in, spread, in_block, normed, acc,
        load_sem, lat_sem, mod_sem, edge_sem, cchain_sem, chain_sem, norm_sem,
    ) = refs
    n, tps, dps = dims
    sp, tp, dp = lax.axis_index("sp"), lax.axis_index("tp"), lax.axis_index("dp")
    place = tp * dps + dp
    places = tps * dps
    width = latent.shape[1]
    half = latent.shape[0]
    length = lat_v.shape[0]
    ctx_len = context.shape[0]
    heads = step_bias.shape[1] // 2
    inner = w_sig.shape[1]
    head_dim = inner // heads
    group_count = w_wr.shape[1] // STATE
    per_group = heads // group_count
    gw = per_group * head_dim
    sw = w_wr.shape[1]
    blocks = length // BLOCK
    mod_rows, mod_cols = shift_w.shape
    out_cols = out.shape[1]

    loads = []

    def load(src, dst):
        c = pltpu.make_async_copy(src, dst, load_sem.at[len(loads)])
        c.start()
        loads.append(c)
        return c

    ld_shift = load(shift_w, mod_w.at[0])
    ld_scale = load(scale_w, mod_w.at[1])
    ld_lat = load(latent, lat_v.at[pl.ds(dp * half, half)])
    ld_ctx = load(context, ctx_v)
    ld_gatew = load(gate_w, mod_w.at[2])
    ld_sig = load(w_sig, w_all.at[:, pl.ds(0, inner)])
    ld_wr = load(w_wr, w_all.at[:, pl.ds(inner, sw)])
    ld_st = load(w_step, w_st)
    ld_rd = load(w_rd, w_all.at[:, pl.ds(inner + sw, sw)])
    ld_gate = load(w_gate, w_all.at[:, pl.ds(inner + 2 * sw, inner)])
    ld_outs = [
        load(w_out.at[pl.ds(q * inner + g * gw, gw)], w_o.at[g, pl.ds(q * gw, gw)])
        for g in range(group_count) for q in range(places)
    ]

    @pl.when(sp == 0)
    def _():
        edge_in[0] = jnp.zeros(edge_in.shape[1:], F32)

    @pl.when(sp == n - 1)
    def _():
        edge_in[1] = jnp.zeros(edge_in.shape[1:], F32)

    barrier = pltpu.get_barrier_semaphore()
    sp_peer = [lax.rem(sp + k, n) for k in range(1, n)]
    tp_peer = [lax.rem(tp + k, tps) for k in range(1, tps)]
    dp_peer = [lax.rem(dp + k, dps) for k in range(1, dps)]
    place_peer = []
    for a in range(tps):
        for b in range(dps):
            if a or b:
                place_peer.append((lax.rem(tp + a, tps), lax.rem(dp + b, dps)))
    for p in sp_peer:
        pl.semaphore_signal(barrier, inc=1, device_id={"sp": p}, device_id_type=MESH)
    for a, b in place_peer:
        pl.semaphore_signal(barrier, inc=1, device_id={"tp": a, "dp": b}, device_id_type=MESH)
    pl.semaphore_wait(barrier, len(sp_peer) + len(place_peer))

    sends = []

    def send(src, dst, ssem, rsem, dev):
        c = pltpu.make_async_remote_copy(
            src_ref=src, dst_ref=dst, send_sem=ssem, recv_sem=rsem,
            device_id=dev, device_id_type=MESH,
        )
        c.start()
        return c

    def arrived(dst, rsem):
        pltpu.make_async_copy(dst, dst, rsem).wait()

    for k, p in enumerate(dp_peer):
        sends.append(send(latent, lat_v.at[pl.ds(dp * half, half)], lat_sem.at[0, k],
                          lat_sem.at[1, dp], {"dp": p}))

    act[...] = jnp.zeros(act.shape, F32)
    act[0:1, :] = silu(cond[...].astype(F32)).astype(BF16).astype(F32)
    act[1:2, :] = silu(ctx_cond[...].astype(F32)).astype(BF16).astype(F32)
    own_act = act[:, pl.ds(pl.multiple_of(sp * mod_rows, 128), mod_rows)].astype(BF16)
    ld_shift.wait()
    mod_part[0:2, :] = dot(own_act, mod_w[0])[0:2]
    ld_scale.wait()
    mod_part[2:4, :] = dot(own_act, mod_w[1])[0:2]
    for k, p in enumerate(sp_peer):
        sends.append(send(mod_part, mod_in.at[sp], mod_sem.at[0, k], mod_sem.at[1, sp], {"sp": p}))
    mod_in[sp] = mod_part[...]
    ld_gatew.wait()
    gate_part[...] = dot(own_act, mod_w[2])[0:1]
    for k, p in enumerate(sp_peer):
        sends.append(send(gate_part, gate_in.at[sp], mod_sem.at[2, k], mod_sem.at[3, sp], {"sp": p}))
    gate_in[sp] = gate_part[...]

    ld_lat.wait()
    ld_ctx.wait()
    for p in dp_peer:
        arrived(lat_v.at[pl.ds(p * half, half)], lat_sem.at[1, p])
    pieces = width // 128
    first_lat = lat_v[0:16, :].astype(F32)[0:1]
    last_lat = lat_v[length - 16:length, :].astype(F32)[15:16]
    first_ctx = ctx_v[0:16, :].astype(F32)[0:1]
    last_ctx = ctx_v[ctx_len - 16:ctx_len, :].astype(F32)[15:16]
    for i in range(pieces):
        cols = slice(i * 128, (i + 1) * 128)
        edge_out[0, 0, i:i + 1, :] = last_lat[:, cols]
        edge_out[0, 1, i:i + 1, :] = last_ctx[:, cols]
        edge_out[1, 0, i:i + 1, :] = first_lat[:, cols]
        edge_out[1, 1, i:i + 1, :] = first_ctx[:, cols]

    def edge_copy(side):
        dev = sp + 1 if side == 0 else sp - 1
        return pltpu.make_async_remote_copy(
            src_ref=edge_out.at[side], dst_ref=edge_in.at[side], send_sem=edge_sem.at[0, side],
            recv_sem=edge_sem.at[1, side], device_id={"sp": dev}, device_id_type=MESH)

    @pl.when(sp < n - 1)
    def _():
        edge_copy(0).start()

    @pl.when(sp > 0)
    def _():
        edge_copy(1).start()

    for p in sp_peer:
        arrived(mod_in.at[p], mod_sem.at[1, p])
    total = mod_in[0]
    for q in range(1, n):
        total = total + mod_in[q]
    mod_sum[...] = total
    for k, (a, b) in enumerate(place_peer):
        sends.append(send(mod_sum, mod_all.at[place], mod_sem.at[4, k], mod_sem.at[5, place],
                          {"tp": a, "dp": b}))
    mod_all[place] = total

    def inv_rms(v):
        return lax.rsqrt(jnp.mean(v * v, axis=-1, keepdims=True) + EPSILON)

    rows_tile = 16

    low_r = lax.broadcasted_iota(jnp.int32, (BLOCK, BLOCK), 0)
    low_c = lax.broadcasted_iota(jnp.int32, (BLOCK, BLOCK), 1)
    lanes2 = 2 * heads
    er = lax.broadcasted_iota(jnp.int32, (lanes2, lanes2 * head_dim), 0)
    ec = lax.broadcasted_iota(jnp.int32, (lanes2, lanes2 * head_dim), 1)
    one = ((ec >= er * head_dim) & (ec < (er + 1) * head_dim)).astype(F32)
    spread[...] = jnp.concatenate([one, one, one], axis=0).astype(BF16)

    def widen(v):
        return jnp.concatenate(thirds(v), axis=1)

    @pl.when(sp > 0)
    def _():
        arrived(edge_in.at[0], edge_sem.at[1, 0])

    @pl.when(sp < n - 1)
    def _():
        arrived(edge_in.at[1], edge_sem.at[1, 1])

    edge_rows[...] = jnp.zeros(edge_rows.shape, F32)
    for i in range(pieces):
        cols = slice(i * 128, (i + 1) * 128)
        edge_rows[0:1, cols] = edge_in[0, 0, i:i + 1, :]
        edge_rows[1:2, cols] = edge_in[1, 0, i:i + 1, :]
        edge_rows[2:3, cols] = edge_in[0, 1, i:i + 1, :]
        edge_rows[3:4, cols] = edge_in[1, 1, i:i + 1, :]

    for a, b in place_peer:
        arrived(mod_all.at[a * dps + b], mod_sem.at[5, a * dps + b])
    for j in range(places):
        cols = slice(j * mod_cols, (j + 1) * mod_cols)
        block_mod = mod_all[j]
        g = gain[0:1, cols]
        for r in range(2):
            shift_rows[r, :, cols] = jnp.broadcast_to(block_mod[r:r + 1], (8, mod_cols))
            scale_rows[r, :, cols] = jnp.broadcast_to((1.0 + block_mod[2 + r:3 + r]) * g, (8, mod_cols))

    def modulated(v, which):
        v3 = v.reshape(-1, 8, width)
        r3 = inv_rms(v).reshape(-1, 8, 1)
        return (v3 * r3 * scale_rows[which][None] + shift_rows[which][None]).reshape(v.shape)

    def ctx_rows(t, carry):
        at = pl.ds(pl.multiple_of(t * rows_tile, rows_tile), rows_tile)
        hid_c[at, :] = modulated(ctx_v[at, :].astype(F32), 1).astype(BF16)
        return carry

    lax.fori_loop(0, ctx_len // rows_tile, ctx_rows, 0)
    edges_lat = modulated(edge_rows[...], 0)
    edges_ctx = modulated(edge_rows[...], 1)
    is_lat = lax.broadcasted_iota(jnp.int32, edges_lat.shape, 0) < 2
    edge_hid = jnp.where(is_lat, edges_lat, edges_ctx)
    hid_c[ctx_len:ctx_len + 16, :] = jnp.concatenate([edge_hid, jnp.zeros_like(edge_hid)], axis=0).astype(BF16)

    ld_sig.wait()
    ld_wr.wait()
    ld_rd.wait()
    conv_tiles = (inner + 2 * sw) // TILE_N
    ridx = lax.broadcasted_iota(jnp.int32, (16, TILE_N), 0)
    has_above = (sp > 0).astype(F32)
    has_below = (sp < n - 1).astype(F32)

    def ctx_proj(t, carry):
        cols = pl.ds(pl.multiple_of(t * TILE_N, TILE_N), TILE_N)
        got = dot(hid_c[...], w_all[:, cols]).astype(BF16).astype(F32)
        raw_c[8:8 + ctx_len, cols] = got[0:ctx_len]
        edges = got[ctx_len:ctx_len + 8]
        raw[0:8, cols] = jnp.broadcast_to(edges[0:1] * has_above, (8, TILE_N))
        raw[8 + length:16 + length, cols] = jnp.broadcast_to(edges[1:2] * has_below, (8, TILE_N))
        raw_c[0:8, cols] = jnp.broadcast_to(edges[2:3] * has_above, (8, TILE_N))
        raw_c[8 + ctx_len:16 + ctx_len, cols] = jnp.broadcast_to(edges[3:4] * has_below, (8, TILE_N))
        return carry

    lax.fori_loop(0, conv_tiles, ctx_proj, 0)
    ld_st.wait()
    ctx_step_in = dot(hid_c[...], w_st[...])[0:ctx_len, 0:lanes2].astype(BF16).astype(F32)

    rates = -jnp.exp(decay_log[...])
    lane = lax.broadcasted_iota(jnp.int32, (1, lanes2), 1)
    forward = lane < heads

    def sums(ld, size):
        r = lax.broadcasted_iota(jnp.int32, (size, size), 0)
        c = lax.broadcasted_iota(jnp.int32, (size, size), 1)
        tri = jnp.concatenate([(r >= c).astype(F32), (r <= c).astype(F32)], axis=0).astype(BF16)
        parts = thirds(ld)
        both = dot(tri, parts[0]) + (dot(tri, parts[1]) + dot(tri, parts[2]))
        return jnp.where(forward, both[:size], both[size:])

    def conv(win, cols, size):
        v = (taps[0:1, cols] * win[7:7 + size] + taps[1:2, cols] * win[8:8 + size]
             + taps[2:3, cols] * win[9:9 + size])
        return silu(v)

    def widened(v, cols):
        return dot(widen(v), spread[:, cols])

    def span_states(sig_g, wr_g, w_f, w_b):
        rhs = jnp.concatenate([sig_g * w_f, sig_g * w_b], axis=1).astype(BF16)
        return lax.dot_general(wr_g, rhs, (((0,), (0,)), ((), ())), preferred_element_type=F32)

    ctx_step = softplus(ctx_step_in + step_bias[...])
    ctx_ld = rates * ctx_step
    ctx_cum = sums(ctx_ld, ctx_len)
    ctx_end = jnp.where(forward, ctx_cum[ctx_len - 1:ctx_len], ctx_cum[0:1])
    ctx_w = jnp.exp(ctx_end - ctx_cum) * ctx_step
    ctx_dec8 = jnp.broadcast_to(jnp.exp(ctx_end), (8, lanes2))
    fwd_all, bwd_all = slice(0, inner), slice(inner, 2 * inner)
    cdf = widened(ctx_dec8, fwd_all)
    cdb = widened(ctx_dec8, bwd_all)
    ctx_states = []
    for g in range(group_count):
        gc = slice(g * gw, (g + 1) * gw)
        bc = slice(inner + g * gw, inner + (g + 1) * gw)
        wc = slice(inner + g * STATE, inner + (g + 1) * STATE)
        sig_g = conv(raw_c[:, gc], gc, ctx_len)
        wr_g = conv(raw_c[:, wc], wc, ctx_len).astype(BF16)
        ctx_states.append(span_states(sig_g, wr_g, widened(ctx_w, gc), widened(ctx_w, bc)))

    def ctx_copy(side):
        dev = sp - 1 if side == 0 else sp + 1
        return [pltpu.make_async_remote_copy(
            src_ref=s.at[side], dst_ref=d.at[side], send_sem=cchain_sem.at[0, side, i],
            recv_sem=cchain_sem.at[1, side, i], device_id={"sp": dev}, device_id_type=MESH)
            for i, (s, d) in enumerate(((ctx_send, ctx_recv), (cdec_send, cdec_recv)))]

    ctx_acc[0] = jnp.concatenate([s[:, :gw] for s in ctx_states], axis=1)
    ctx_acc[1] = jnp.concatenate([s[:, gw:] for s in ctx_states], axis=1)
    ctx_dec[0] = cdf
    ctx_dec[1] = cdb
    ctx_starts = (n - 1, 0)
    for side in range(2):
        @pl.when(sp == ctx_starts[side])
        def _():
            ctx_send[side] = ctx_acc[side].astype(BF16)
            cdec_send[side] = ctx_dec[side]
            if n > 1:
                for c in ctx_copy(side):
                    c.start()

    def lat_rows(t, carry):
        at = pl.ds(pl.multiple_of(t * rows_tile, rows_tile), rows_tile)
        hid[at, :] = modulated(lat_v[at, :].astype(F32), 0).astype(BF16)
        return carry

    lax.fori_loop(0, length // rows_tile, lat_rows, 0)
    ld_gate.wait()

    def lat_proj(t, carry):
        cols = pl.ds(pl.multiple_of(t * TILE_N, TILE_N), TILE_N)
        raw[8:8 + length, cols] = dot(hid[...], w_all[:, cols]).astype(BF16).astype(F32)
        return carry

    state_tiles = (inner + sw) // TILE_N
    all_tiles = (2 * inner + 2 * sw) // TILE_N

    def ctx_hop(hop):
        for side in range(2):
            @pl.when(sp == (n - 1 - hop if side == 0 else hop))
            def _():
                arrived(ctx_recv.at[side], cchain_sem.at[1, side, 0])
                arrived(cdec_recv.at[side], cchain_sem.at[1, side, 1])
                ctx_acc[side] = (ctx_recv[side].astype(F32)
                                 + cdec_recv[side, 0:1] * ctx_acc[side])
                if hop < n - 1:
                    ctx_send[side] = ctx_acc[side].astype(BF16)
                    cdec_send[side] = cdec_recv[side] * ctx_dec[side]
                    for c in ctx_copy(side):
                        c.start()

    st_raw[...] = dot(hid[...], w_st[...]).astype(BF16).astype(F32)
    if n > 1:
        ctx_hop(1)
    lax.fori_loop(0, state_tiles, lat_proj, 0)
    for hop in range(2, n):
        ctx_hop(hop)

    def lat_block(b, carry):
        at = pl.ds(pl.multiple_of(b * BLOCK, BLOCK), BLOCK)
        window = pl.ds(pl.multiple_of(b * BLOCK, BLOCK), BLOCK + 16)
        step = softplus(st_raw[at, 0:lanes2] + step_bias[...])
        ld = rates * step + extra[:, at].T
        cum = sums(ld, BLOCK)
        end = jnp.where(forward, cum[BLOCK - 1:BLOCK], cum[0:1])
        weight = jnp.exp(end - cum) * step
        cum_col[b] = cum
        ecum_col[b] = jnp.exp(cum)
        cum_row[b] = cum.T
        step_row[b] = step.T
        end8 = jnp.broadcast_to(jnp.exp(end), (8, lanes2))
        dec[b] = widened(end8, slice(0, 2 * inner))
        for g in range(group_count):
            gc = slice(g * gw, (g + 1) * gw)
            bc = slice(inner + g * gw, inner + (g + 1) * gw)
            wc = slice(inner + g * STATE, inner + (g + 1) * STATE)
            sig_g = conv(raw[window, gc], gc, BLOCK)
            wr_g = conv(raw[window, wc], wc, BLOCK).astype(BF16)
            sig[at, gc] = sig_g.astype(BF16)
            wr[at, g * STATE:(g + 1) * STATE] = wr_g
            states[b, g] = span_states(sig_g, wr_g, widened(weight, gc), widened(weight, bc))
        return carry

    lax.fori_loop(0, blocks, lat_block, 0)

    def group_cols(side, g):
        return slice(side * inner + g * gw, side * inner + (g + 1) * gw)

    def block_at(side, i):
        return i if side == 0 else blocks - 1 - i

    def side_cols(side):
        return slice(side * gw, (side + 1) * gw)

    for g in range(group_count):
        for side in range(2):
            def total_step(i, run):
                b = block_at(side, i)
                return run * dec[b, 0:1, group_cols(side, g)] + states[b, g, :, side_cols(side)]

            span_total[side, g] = lax.fori_loop(0, blocks, total_step, jnp.zeros((STATE, gw), F32))
    dec_all = dec[0]
    for b in range(1, blocks):
        dec_all = dec_all * dec[b]

    def chain_copy(side, g):
        dev = sp + 1 if side == 0 else sp - 1
        return pltpu.make_async_remote_copy(
            src_ref=chain_out.at[side, g], dst_ref=chain_in.at[side, g],
            send_sem=chain_sem.at[0, side, g], recv_sem=chain_sem.at[1, side, g],
            device_id={"sp": dev}, device_id_type=MESH)

    def chain_hop(hop):
        for side in range(2):
            for g in range(group_count):
                @pl.when(sp == (hop if side == 0 else n - 1 - hop))
                def _():
                    if hop == 0:
                        chain_in[side, g] = ctx_acc[side, :, g * gw:(g + 1) * gw].astype(BF16)
                    else:
                        arrived(chain_in.at[side, g], chain_sem.at[1, side, g])
                    if hop < n - 1:
                        chain_out[side, g] = (
                            chain_in[side, g].astype(F32) * dec_all[0:1, group_cols(side, g)]
                            + span_total[side, g]).astype(BF16)
                        chain_copy(side, g).start()

    def reader_block(b, carry):
        window = pl.ds(pl.multiple_of(b * BLOCK, BLOCK), BLOCK + 16)
        at = pl.ds(pl.multiple_of(b * BLOCK, BLOCK), BLOCK)
        cr, sr, cc = cum_row[b], step_row[b], cum_col[b]
        lane_g = lax.broadcasted_iota(jnp.int32, (BLOCK, gw), 1)
        for g in range(group_count):
            gc = slice(g * gw, (g + 1) * gw)
            rc = slice(inner + sw + g * STATE, inner + sw + (g + 1) * STATE)
            rd_g = conv(raw[window, rc], rc, BLOCK).astype(BF16)
            rd[at, g * STATE:(g + 1) * STATE] = rd_g
            wr_g = wr[at, g * STATE:(g + 1) * STATE]
            sig_g = sig[at, gc]
            pair = lax.dot_general(rd_g, wr_g, (((1,), (1,)), ((), ())), preferred_element_type=F32)
            mixes, sigs = [], []
            for e in range(per_group):
                f, k = g * per_group + e, heads + g * per_group + e
                gap = jnp.where(low_r >= low_c, cc[:, f:f + 1] - cr[f:f + 1], cc[:, k:k + 1] - cr[k:k + 1])
                sf, sk = sr[f:f + 1], sr[k:k + 1]
                size = jnp.where(low_r > low_c, sf, jnp.where(low_r < low_c, sk, sf + sk))
                mixes.append((jnp.exp(gap) * size * pair).astype(BF16))
                mine = (lane_g >= e * head_dim) & (lane_g < (e + 1) * head_dim)
                sigs.append(jnp.where(mine, sig_g, jnp.zeros_like(sig_g)))
            in_block[at, gc] = dot(jnp.concatenate(mixes, axis=1), jnp.concatenate(sigs, axis=0))
        return carry

    chain_hop(0)
    lax.fori_loop(state_tiles, all_tiles - 1, lat_proj, 0)
    if n > 1:
        chain_hop(1)
    lax.fori_loop(all_tiles - 1, all_tiles, lat_proj, 0)
    if n > 2:
        chain_hop(2)
    lax.fori_loop(0, blocks, reader_block, 0)
    for hop in range(3, n):
        chain_hop(hop)

    for p in sp_peer:
        arrived(gate_in.at[p], mod_sem.at[3, p])
    gate_vec = gate_in[0]
    for q in range(1, n):
        gate_vec = gate_vec + gate_in[q]

    chunk = pl.ds(pl.multiple_of(place * gw, 128), gw)

    def norm_copy(g, b, cols, dev, slot, sender):
        ref = normed.at[g, pl.ds(pl.multiple_of(b * BLOCK, BLOCK), BLOCK), cols]
        return pltpu.make_async_remote_copy(
            src_ref=ref, dst_ref=ref, send_sem=norm_sem.at[0, slot, g, b],
            recv_sem=norm_sem.at[1, sender, g, b], device_id=dev, device_id_type=MESH)

    def place_cols(q):
        return pl.ds(pl.multiple_of(q * gw, 128), gw)

    for g in range(group_count):
        gc = slice(g * gw, (g + 1) * gw)
        for side in range(2):
            def enter(i, run):
                b = block_at(side, i)
                ent[b, g, :, side_cols(side)] = run.astype(BF16)
                return run * dec[b, 0:1, group_cols(side, g)] + states[b, g, :, side_cols(side)]

            lax.fori_loop(0, blocks, enter, chain_in[side, g].astype(F32))

        def finish(b, carry):
            at = pl.ds(pl.multiple_of(b * BLOCK, BLOCK), BLOCK)
            at8 = pl.ds(pl.multiple_of(b * BLOCK, BLOCK) + 8, BLOCK)
            carried = dot(rd[at, g * STATE:(g + 1) * STATE], ent[b, g])
            grown = widen(ecum_col[b])
            both = (in_block[at, gc]
                    + carried[:, :gw] * dot(grown, spread[:, group_cols(0, g)])
                    + carried[:, gw:] * dot(grown, spread[:, group_cols(1, g)]))
            start = 1 * inner + 2 * sw + g * gw
            gated = both * silu(raw[at8, start:start + gw])
            done = gated * inv_rms(gated) * group_gain[0:1, gc]
            normed[g, at, chunk] = done.astype(BF16)
            for k, a in enumerate(tp_peer):
                norm_copy(g, b, chunk, {"tp": a}, k, place).start()
            for k, p in enumerate(dp_peer):
                norm_copy(g, b, chunk, {"dp": p}, tps - 1 + k, place).start()
            return carry

        lax.fori_loop(0, blocks, finish, 0)

    for c in ld_outs:
        c.wait()
    own_out = pl.ds(pl.multiple_of(place * out_cols, 128), out_cols)
    slots = (tps - 1) + (dps - 1)
    for g in range(group_count):
        def project(b, carry):
            at = pl.ds(pl.multiple_of(b * BLOCK, BLOCK), BLOCK)
            for k, a in enumerate(tp_peer):
                q = a * dps + dp
                norm_copy(g, b, place_cols(q), {"tp": a}, 0, q).wait_recv()
                for j, p in enumerate(dp_peer):
                    slot = slots + k * (dps - 1) + j
                    norm_copy(g, b, place_cols(q), {"dp": p}, slot, q).start()
            for p in dp_peer:
                for a in range(tps):
                    q = a * dps + p
                    norm_copy(g, b, place_cols(q), {"dp": p}, 0, q).wait_recv()
            part = dot(normed[g, at, :], w_o[g])
            if g > 0:
                part = part + acc[at, :]
            if g < group_count - 1:
                acc[at, :] = part
            else:
                kept = lat_v[at, own_out].astype(F32)
                out[at, :] = (kept + gate_vec * part).astype(BF16)
            return carry

        lax.fori_loop(0, blocks, project, 0)

    for c in sends:
        c.wait_send()

    @pl.when(sp < n - 1)
    def _():
        edge_copy(0).wait_send()

    @pl.when(sp > 0)
    def _():
        edge_copy(1).wait_send()

    for side in range(2):
        @pl.when(sp != ctx_starts[1 - side])
        def _():
            for c in ctx_copy(side):
                c.wait_send()

        @pl.when(sp != ctx_starts[side])
        def _():
            for g in range(group_count):
                chain_copy(side, g).wait_send()

    for g in range(group_count):
        def drained(b, carry):
            for k, a in enumerate(tp_peer):
                norm_copy(g, b, chunk, {"tp": a}, k, place).wait_send()
            for k, p in enumerate(dp_peer):
                norm_copy(g, b, chunk, {"dp": p}, tps - 1 + k, place).wait_send()
            for k, a in enumerate(tp_peer):
                for j, p in enumerate(dp_peer):
                    slot = slots + k * (dps - 1) + j
                    norm_copy(g, b, place_cols(a * dps + dp), {"dp": p}, slot, place).wait_send()
            return carry

        lax.fori_loop(0, blocks, drained, 0)


def on_device(dims, *args):
    (
        latent, context, condition, context_condition, shift_weight, scale_weight, gate_weight,
        norm_gain, out_gate_weight, signal_weight, writer_weight, reader_matrix, step_weight,
        signal_taps, writer_taps, reader_taps, step_bias, decay_log, decay_extra, group_gain,
        output_weight,
    ) = args
    n, tps, dps = dims
    half, width = latent.shape
    length = half * dps
    ctx_len = context.shape[0]
    heads = step_bias.shape[1]
    inner = signal_weight.shape[1]
    sw = writer_weight.shape[1]
    groups = sw // STATE
    gw = inner // groups
    blocks = length // BLOCK
    places = tps * dps
    mod_rows, mod_cols = shift_weight.shape
    out_cols = output_weight.shape[1]
    lanes2 = 2 * heads
    conv_cols = inner + 2 * sw
    steps = jnp.concatenate([step_weight[0], step_weight[1]], axis=1)
    steps = jnp.pad(steps, ((0, 0), (0, 128 - lanes2)))
    taps = jnp.concatenate([signal_taps, writer_taps, reader_taps], axis=1)
    hbm = pl.BlockSpec(memory_space=pl.ANY)
    vmem = pl.BlockSpec(memory_space=pltpu.VMEM)
    slots = (tps - 1) + (dps - 1) + (tps - 1) * (dps - 1)
    peers = max(n - 1, places - 1, 1)
    scratch = [
        pltpu.VMEM((length, width), BF16),
        pltpu.VMEM((ctx_len, width), BF16),
        pltpu.VMEM((8, width), F32),
        pltpu.VMEM((3, mod_rows, mod_cols), BF16),
        pltpu.VMEM((4, mod_cols), F32),
        pltpu.VMEM((1, mod_cols), F32),
        pltpu.VMEM((n, 4, mod_cols), F32),
        pltpu.VMEM((n, 1, mod_cols), F32),
        pltpu.VMEM((4, mod_cols), F32),
        pltpu.VMEM((places, 4, mod_cols), F32),
        pltpu.VMEM((2, 8, width), F32),
        pltpu.VMEM((2, 8, width), F32),
        pltpu.VMEM((2, 2, width // 128, 128), F32),
        pltpu.VMEM((2, 2, width // 128, 128), F32),
        pltpu.VMEM((8, width), F32),
        pltpu.VMEM((length, width), BF16),
        pltpu.VMEM((ctx_len + 16, width), BF16),
        pltpu.VMEM((width, 2 * inner + 2 * sw), BF16),
        pltpu.VMEM((width, 128), BF16),
        pltpu.VMEM((groups, places * gw, out_cols), BF16),
        pltpu.VMEM((length + 16, 2 * inner + 2 * sw), F32),
        pltpu.VMEM((ctx_len + 16, conv_cols), F32),
        pltpu.VMEM((length, 128), F32),
        pltpu.VMEM((blocks, BLOCK, lanes2), F32),
        pltpu.VMEM((blocks, BLOCK, lanes2), F32),
        pltpu.VMEM((blocks, lanes2, BLOCK), F32),
        pltpu.VMEM((blocks, lanes2, BLOCK), F32),
        pltpu.VMEM((length, inner), BF16),
        pltpu.VMEM((length, sw), BF16),
        pltpu.VMEM((length, sw), BF16),
        pltpu.VMEM((blocks, groups, STATE, 2 * gw), F32),
        pltpu.VMEM((blocks, 8, 2 * inner), F32),
        pltpu.VMEM((blocks, groups, STATE, 2 * gw), BF16),
        pltpu.VMEM((2, STATE, inner), F32),
        pltpu.VMEM((2, 8, inner), F32),
        pltpu.VMEM((2, STATE, inner), BF16),
        pltpu.VMEM((2, STATE, inner), BF16),
        pltpu.VMEM((2, 8, inner), F32),
        pltpu.VMEM((2, 8, inner), F32),
        pltpu.VMEM((2, groups, STATE, gw), F32),
        pltpu.VMEM((2, groups, STATE, gw), BF16),
        pltpu.VMEM((2, groups, STATE, gw), BF16),
        pltpu.VMEM((3 * lanes2, 2 * inner), BF16),
        pltpu.VMEM((length, inner), F32),
        pltpu.VMEM((groups, length, places * gw), BF16),
        pltpu.VMEM((length, out_cols), F32),
        pltpu.SemaphoreType.DMA((10 + groups * places,)),
        pltpu.SemaphoreType.DMA((2, dps)),
        pltpu.SemaphoreType.DMA((6, max(n, places))),
        pltpu.SemaphoreType.DMA((2, 2)),
        pltpu.SemaphoreType.DMA((2, 2, 2)),
        pltpu.SemaphoreType.DMA((2, 2, groups)),
        pltpu.SemaphoreType.DMA((2, max(slots, places), groups, blocks)),
    ]
    specs = [hbm, hbm, vmem, vmem, hbm, hbm, hbm, vmem, hbm, hbm, hbm, hbm, hbm,
             vmem, vmem, vmem, vmem, vmem, hbm]
    return pl.pallas_call(
        functools.partial(kernel, dims),
        out_shape=jax.ShapeDtypeStruct((length, out_cols), BF16),
        in_specs=specs,
        out_specs=vmem,
        scratch_shapes=scratch,
        compiler_params=pltpu.CompilerParams(
            collective_id=0, has_side_effects=True, vmem_limit_bytes=67043328),
    )(
        latent, context, condition.reshape(1, -1), context_condition.reshape(1, -1), shift_weight,
        scale_weight, gate_weight, norm_gain.reshape(1, -1), out_gate_weight, signal_weight,
        writer_weight, reader_matrix, steps, taps, step_bias.reshape(1, lanes2),
        decay_log.reshape(1, lanes2), decay_extra.reshape(lanes2, length),
        group_gain.reshape(1, -1), output_weight,
    )


def solution(mesh):
    dims = (mesh.shape["sp"], mesh.shape["tp"], mesh.shape["dp"])
    in_specs = (
        P(("grp", "sp", "dp"), None),
        P(("grp", "sp"), None),
        P("grp"),
        P(),
        P("sp", ("tp", "dp")),
        P("sp", ("tp", "dp")),
        P("sp", ("tp", "dp")),
        P(),
        P(None, ("tp", "dp")),
        P(None, ("tp", "dp")),
        P(None, ("tp", "dp")),
        P(None, ("tp", "dp")),
        P(None, None, ("tp", "dp")),
        P(None, ("tp", "dp")),
        P(None, ("tp", "dp")),
        P(None, ("tp", "dp")),
        P(None, ("tp", "dp")),
        P(None, ("tp", "dp")),
        P(None, ("tp", "dp"), ("grp", "sp")),
        P(("tp", "dp")),
        P(None, ("tp", "dp")),
    )
    out_specs = P(("grp", "sp"), ("tp", "dp"))
    return jax.shard_map(
        functools.partial(on_device, dims), mesh=mesh, in_specs=in_specs, out_specs=out_specs,
        check_vma=False,
    )
```

profile of v0, /device:TPU:0, one launch (start us, length us, event | category | flops | bytes accessed | tf_op | source)
XLA Modules:
  0.0 93.3 jit_solution(3606230426791345244)
XLA Ops:
  0.0 1.2 %reshape.24.refs_14_ = f32[1,16]{1,0:T(1,128)} reshape(f32[2,8]{1,0:T(2,128)} %param.37) | data formatting | bytes 128 | tf_op jit(solution)/shard_map/reshape | solution.py:688
  1.2 1.4 %reshape.25.refs_15_ = f32[1,16]{1,0:T(1,128)} reshape(f32[2,8]{1,0:T(2,128)} %param.38) | data formatting | bytes 128 | tf_op jit(solution)/shard_map/reshape | solution.py:689
  2.6 1.3 %reshape.21.refs_2_ = bf16[1,4096]{1,0:T(2,128)(2,1)} reshape(bf16[4096]{0:T(1024)(128)(2,1)} %param.23) | data formatting | bytes 16384 | tf_op jit(solution)/shard_map/reshape | solution.py:686
  3.9 1.3 %reshape.22.refs_3_ = bf16[1,4096]{1,0:T(2,128)(2,1)} reshape(bf16[4096]{0:T(1024)(128)(2,1)} %param.24) | data formatting | bytes 16384 | tf_op jit(solution)/shard_map/reshape | solution.py:686
  5.2 1.3 %pad_maximum_fusion.1.refs_13_ = f32[3,1024]{1,0:T(4,128)} fusion(f32[3,256]{1,0:T(4,128)} %param.36, f32[3,256]{1,0:T(4,128)} %param.35, f32[3,512]{1,0:T(4,128)} %param.34), kind=kLoop, calls=%fused_computation.3 | loop fusion | flops 6144 | bytes 24576 | tf_op jit(solution)/shard_map/concatenate | solution.py:615
  6.5 0.9 slice_bitcast_fusion.1
  7.4 0.5 copy.24
  7.9 1.2 %pad.4.refs_12_ = bf16[4096,128]{1,0:T(8,128)(2,1)} pad(bf16[4096,16]{1,0:T(8,128)(2,1)S(1)} %copy.24, bf16[]{:T(256)} %constant.2.clone.1), padding=0_0x0_112 | pad | bytes 1179650 | tf_op jit(solution)/shard_map/jit(_pad)/pad | solution.py:614
  9.1 81.6 %shard_map.199 = bf16[768,1024]{1,0:T(8,128)(2,1)} custom-call(bf16[384,4096]{1,0:T(8,128)(2,1)} %refs_0_.1, bf16[128,4096]{1,0:T(8,128)(2,1)} %refs_1_.1, bf16[1,4096]{1,0:T(2,128)(2,1)} %reshape.21.refs_2_, bf16[1,4096]{1,0:T(2,128)(2,1)} %reshape.22.refs_3_, bf16[1024,1024]{1,0:T(8,128)(2,1)} %refs_4_.1, bf16[1024,1024]{1,0:T(8,128)(2,1)} %refs_5_.1, ...), custom_call_target="tpu_custom_call" | custom-call | tf_op jit(solution)/shard_map/pallas_call | solution.py:677
  90.6 2.7 %copy.26 = bf16[768,1024]{1,0:T(8,128)(2,1)} copy(bf16[768,1024]{1,0:T(8,128)(2,1)} %shard_map.199) | data formatting | bytes 3145728
  (1 shorter events, 0.0 us)
where the time goes:
time: 93.8 us; the launch traced here: 93.3 us
  Pallas kernels  81.6 us (87%)
  local copies, waits for them, and re-layouts  10.4 us (11%)
  other arithmetic  1.34 us (1%)
    pallas_call x1, Pallas kernels, on_device(): pl.pallas_call(functools.partial(kernel, dims), out_shape=jax.ShapeDtypeS...  81.6 us
    unnamed x1, local copies, waits for them, and re-layouts  2.67 us

commit v1 on v0

v1 whole, which is shorter than its diff:
```python
import functools

import jax
import jax.numpy as jnp
from jax import lax
from jax.experimental import pallas as pl
from jax.experimental.pallas import tpu as pltpu
from jax.sharding import PartitionSpec as P

STATE = 128
BLOCK = 128
EPSILON = 1e-06
TILE_N = 512
F32 = jnp.float32
BF16 = jnp.bfloat16
MESH = pl.DeviceIdType.MESH


def silu(v):
    return v / (1.0 + jnp.exp(-v))


def softplus(v):
    return jnp.maximum(v, 0.0) + jnp.log1p(jnp.exp(-jnp.abs(v)))


def dot(a, b):
    return jnp.dot(a, b, preferred_element_type=F32)


def dot_t(a, b):
    return lax.dot_general(a, b, (((1,), (1,)), ((), ())), preferred_element_type=F32)


def thirds(v):
    first = v.astype(BF16)
    rest = v - first.astype(F32)
    second = rest.astype(BF16)
    third = (rest - second.astype(F32)).astype(BF16)
    return first, second, third


def kernel(dims, *refs):
    (
        latent, context, cond, ctx_cond, shift_w, scale_w, gate_w, gain,
        w_gate, w_sig, w_wr, w_rd, w_step, sig_taps, wr_taps, rd_taps, step_bias, decay_log, extra,
        group_gain, w_out, out,
        lat_v, ctx_v, act, mod_w, mod_part, gate_part, mod_in, gate_in, mod_sum, mod_all,
        scale_rows, shift_rows, edge_out, edge_in, edge_rows, hid, hid_c, w_all, w_st, w_o,
        raw, raw_c, gates, lat_rms, ctx_rms, cum_col, ecum_col, weight_col, cum_row, step_row, sig, wr, rd,
        states, dec, ent, ctx_acc, ctx_dec, ctx_send, ctx_recv, cdec_send, cdec_recv,
        span_total, chain_out, chain_in, spread, in_block, normed, acc,
        load_sem, lat_sem, mod_sem, edge_sem, cchain_sem, chain_sem, norm_sem,
    ) = refs
    n, tps, dps = dims
    sp, tp, dp = lax.axis_index("sp"), lax.axis_index("tp"), lax.axis_index("dp")
    place = tp * dps + dp
    places = tps * dps
    width = latent.shape[1]
    half = latent.shape[0]
    length = lat_v.shape[0]
    ctx_len = context.shape[0]
    heads = step_bias.shape[1]
    inner = w_sig.shape[1]
    head_dim = inner // heads
    group_count = w_wr.shape[1] // STATE
    per_group = heads // group_count
    gw = per_group * head_dim
    sw = w_wr.shape[1]
    blocks = length // BLOCK
    mod_rows, mod_cols = shift_w.shape
    out_cols = out.shape[1]

    loads = []

    def load(src, dst):
        c = pltpu.make_async_copy(src, dst, load_sem.at[len(loads)])
        c.start()
        loads.append(c)
        return c

    ld_shift = load(shift_w, mod_w.at[0])
    ld_scale = load(scale_w, mod_w.at[1])
    ld_lat = load(latent, lat_v.at[pl.ds(dp * half, half)])
    ld_ctx = load(context, ctx_v)
    ld_gatew = load(gate_w, mod_w.at[2])
    ld_sig = load(w_sig, w_all.at[:, pl.ds(sw, inner)])
    ld_wr = load(w_wr, w_all.at[:, pl.ds(0, sw)])
    ld_st = load(w_step, w_st)
    ld_rd = load(w_rd, w_all.at[:, pl.ds(inner + sw, sw)])
    ld_gate = load(w_gate, w_all.at[:, pl.ds(inner + 2 * sw, inner)])
    ld_outs = [
        load(w_out.at[pl.ds(q * inner + g * gw, gw)], w_o.at[g, pl.ds(q * gw, gw)])
        for g in range(group_count) for q in range(places)
    ]

    @pl.when(sp == 0)
    def _():
        edge_in[0] = jnp.zeros(edge_in.shape[1:], F32)

    @pl.when(sp == n - 1)
    def _():
        edge_in[1] = jnp.zeros(edge_in.shape[1:], F32)

    barrier = pltpu.get_barrier_semaphore()
    sp_peer = [lax.rem(sp + k, n) for k in range(1, n)]
    tp_peer = [lax.rem(tp + k, tps) for k in range(1, tps)]
    dp_peer = [lax.rem(dp + k, dps) for k in range(1, dps)]
    place_peer = []
    for a in range(tps):
        for b in range(dps):
            if a or b:
                place_peer.append((lax.rem(tp + a, tps), lax.rem(dp + b, dps)))
    for p in sp_peer:
        pl.semaphore_signal(barrier, inc=1, device_id={"sp": p}, device_id_type=MESH)
    for a, b in place_peer:
        pl.semaphore_signal(barrier, inc=1, device_id={"tp": a, "dp": b}, device_id_type=MESH)
    sends = []

    def send(src, dst, ssem, rsem, dev):
        c = pltpu.make_async_remote_copy(
            src_ref=src, dst_ref=dst, send_sem=ssem, recv_sem=rsem,
            device_id=dev, device_id_type=MESH,
        )
        c.start()
        return c

    def arrived(dst, rsem):
        pltpu.make_async_copy(dst, dst, rsem).wait()

    act[...] = jnp.zeros(act.shape, F32)
    act[0:1, :] = silu(cond[...].astype(F32)).astype(BF16).astype(F32).reshape(1, -1)
    act[1:2, :] = silu(ctx_cond[...].astype(F32)).astype(BF16).astype(F32).reshape(1, -1)
    own_act = act[:, pl.ds(pl.multiple_of(sp * mod_rows, 128), mod_rows)].astype(BF16)
    ld_shift.wait()
    mod_part[0:2, :] = dot(own_act, mod_w[0])[0:2]
    ld_scale.wait()
    mod_part[2:4, :] = dot(own_act, mod_w[1])[0:2]
    pl.semaphore_wait(barrier, len(sp_peer) + len(place_peer))
    for k, p in enumerate(sp_peer):
        sends.append(send(mod_part, mod_in.at[sp], mod_sem.at[0, k], mod_sem.at[1, sp], {"sp": p}))
    mod_in[sp] = mod_part[...]

    for k, p in enumerate(dp_peer):
        sends.append(send(latent, lat_v.at[pl.ds(dp * half, half)], lat_sem.at[0, k],
                          lat_sem.at[1, dp], {"dp": p}))

    def inv_rms(v):
        return lax.rsqrt(jnp.mean(v * v, axis=-1, keepdims=True) + EPSILON)

    def row_tile(rows):
        return min(rows, 64)

    def rms_rows(ref, keep, start, count):
        tile = row_tile(count)

        def step(t, carry):
            at = pl.ds(pl.multiple_of(start + t * tile, tile), tile)
            total = jnp.zeros((tile, 128), F32)
            for c in range(width // 128):
                v = ref[at, c * 128:(c + 1) * 128].astype(F32)
                total = total + v * v
            mean = jnp.sum(total, axis=-1, keepdims=True) * (1.0 / width)
            keep[at, :] = jnp.broadcast_to(lax.rsqrt(mean + EPSILON), (tile, 128))
            return carry

        lax.fori_loop(0, count // tile, step, 0)

    ld_lat.wait()
    rms_rows(lat_v, lat_rms, dp * half, half)

    for p in sp_peer:
        arrived(mod_in.at[p], mod_sem.at[1, p])
    total = mod_in[0]
    for q in range(1, n):
        total = total + mod_in[q]
    mod_sum[...] = total
    for k, (a, b) in enumerate(place_peer):
        sends.append(send(mod_sum, mod_all.at[place], mod_sem.at[4, k], mod_sem.at[5, place],
                          {"tp": a, "dp": b}))
    mod_all[place] = total

    ld_ctx.wait()
    for p in dp_peer:
        arrived(lat_v.at[pl.ds(p * half, half)], lat_sem.at[1, p])
    pieces = width // 128
    first_lat = lat_v[0:16, :].astype(F32)[0:1]
    last_lat = lat_v[length - 16:length, :].astype(F32)[15:16]
    first_ctx = ctx_v[0:16, :].astype(F32)[0:1]
    last_ctx = ctx_v[ctx_len - 16:ctx_len, :].astype(F32)[15:16]
    for i in range(pieces):
        cols = slice(i * 128, (i + 1) * 128)
        edge_out[0, 0, i:i + 1, :] = last_lat[:, cols]
        edge_out[0, 1, i:i + 1, :] = last_ctx[:, cols]
        edge_out[1, 0, i:i + 1, :] = first_lat[:, cols]
        edge_out[1, 1, i:i + 1, :] = first_ctx[:, cols]

    def edge_copy(side):
        dev = sp + 1 if side == 0 else sp - 1
        return pltpu.make_async_remote_copy(
            src_ref=edge_out.at[side], dst_ref=edge_in.at[side], send_sem=edge_sem.at[0, side],
            recv_sem=edge_sem.at[1, side], device_id={"sp": dev}, device_id_type=MESH)

    @pl.when(sp < n - 1)
    def _():
        edge_copy(0).start()

    @pl.when(sp > 0)
    def _():
        edge_copy(1).start()

    for p in dp_peer:
        rms_rows(lat_v, lat_rms, p * half, half)
    rms_rows(ctx_v, ctx_rms, 0, ctx_len)
    ld_gatew.wait()
    gate_part[...] = dot(own_act, mod_w[2])[0:1]
    for k, p in enumerate(sp_peer):
        sends.append(send(gate_part, gate_in.at[sp], mod_sem.at[2, k], mod_sem.at[3, sp], {"sp": p}))
    gate_in[sp] = gate_part[...]

    low_r = lax.broadcasted_iota(jnp.int32, (BLOCK, BLOCK), 0)
    low_c = lax.broadcasted_iota(jnp.int32, (BLOCK, BLOCK), 1)
    lanes2 = 2 * heads
    er = lax.broadcasted_iota(jnp.int32, (lanes2, lanes2 * head_dim), 0)
    ec = lax.broadcasted_iota(jnp.int32, (lanes2, lanes2 * head_dim), 1)
    one = ((ec >= er * head_dim) & (ec < (er + 1) * head_dim)).astype(F32)
    spread[...] = jnp.concatenate([one, one, one], axis=0).astype(BF16)

    def widen(v):
        return jnp.concatenate(thirds(v), axis=1)

    for a, b in place_peer:
        arrived(mod_all.at[a * dps + b], mod_sem.at[5, a * dps + b])
    for j in range(places):
        cols = slice(j * mod_cols, (j + 1) * mod_cols)
        block_mod = mod_all[j]
        g = gain[0:1, cols]
        for r in range(2):
            shift_rows[r, :, cols] = jnp.broadcast_to(block_mod[r:r + 1], (8, mod_cols))
            scale_rows[r, :, cols] = jnp.broadcast_to((1.0 + block_mod[2 + r:3 + r]) * g, (8, mod_cols))

    def hidden_rows(ref, keep, goal, which, start, count):
        tile = row_tile(count)

        def step(t, carry):
            at = pl.ds(pl.multiple_of(start + t * tile, tile), tile)
            r3 = keep[at, :].reshape(tile // 8, 8, 128)
            for c in range(width // 128):
                cols = slice(c * 128, (c + 1) * 128)
                v = ref[at, cols].astype(F32).reshape(tile // 8, 8, 128)
                h = v * r3 * scale_rows[which, :, cols][None] + shift_rows[which, :, cols][None]
                goal[at, cols] = h.reshape(tile, 128).astype(BF16)
            return carry

        lax.fori_loop(0, count // tile, step, 0)

    hidden_rows(ctx_v, ctx_rms, hid_c, 1, 0, ctx_len)

    @pl.when(sp > 0)
    def _():
        arrived(edge_in.at[0], edge_sem.at[1, 0])

    @pl.when(sp < n - 1)
    def _():
        arrived(edge_in.at[1], edge_sem.at[1, 1])

    edge_rows[...] = jnp.zeros(edge_rows.shape, F32)
    for i in range(pieces):
        cols = slice(i * 128, (i + 1) * 128)
        edge_rows[0:1, cols] = edge_in[0, 0, i:i + 1, :]
        edge_rows[1:2, cols] = edge_in[1, 0, i:i + 1, :]
        edge_rows[2:3, cols] = edge_in[0, 1, i:i + 1, :]
        edge_rows[3:4, cols] = edge_in[1, 1, i:i + 1, :]
    edge_v = edge_rows[...]
    edge_n = edge_v * inv_rms(edge_v)
    is_lat = lax.broadcasted_iota(jnp.int32, edge_v.shape, 0) < 2
    edge_hid = jnp.where(is_lat, edge_n * scale_rows[0] + shift_rows[0],
                         edge_n * scale_rows[1] + shift_rows[1])
    hid_c[ctx_len:ctx_len + 16, :] = jnp.concatenate([edge_hid, jnp.zeros_like(edge_hid)], axis=0).astype(BF16)

    ld_sig.wait()
    ld_wr.wait()
    ld_rd.wait()
    has_above = (sp > 0).astype(F32)
    has_below = (sp < n - 1).astype(F32)

    def ctx_proj(t, carry):
        cols = pl.ds(pl.multiple_of(t * TILE_N, TILE_N), TILE_N)
        got = dot(hid_c[...], w_all[:, cols]).astype(BF16).astype(F32)
        for i in range(TILE_N // 128):
            c, piece = t * (TILE_N // 128) + i, got[:, i * 128:(i + 1) * 128]
            raw_c[c, 8:8 + ctx_len, :] = piece[0:ctx_len]
            edges = piece[ctx_len:ctx_len + 8]
            raw[c, 0:8, :] = jnp.broadcast_to(edges[0:1] * has_above, (8, 128))
            raw[c, 8 + length:16 + length, :] = jnp.broadcast_to(edges[1:2] * has_below, (8, 128))
            raw_c[c, 0:8, :] = jnp.broadcast_to(edges[2:3] * has_above, (8, 128))
            raw_c[c, 8 + ctx_len:16 + ctx_len, :] = jnp.broadcast_to(edges[3:4] * has_below, (8, 128))
        return carry

    lax.fori_loop(0, (inner + 2 * sw) // TILE_N, ctx_proj, 0)
    ld_st.wait()
    ctx_step_in = dot_t(hid_c[0:ctx_len], w_st[...]).astype(BF16).astype(F32)

    bias = jnp.concatenate([step_bias[0:1], step_bias[1:2]], axis=1)
    rates = -jnp.exp(jnp.concatenate([decay_log[0:1], decay_log[1:2]], axis=1))

    def sums(ld, size):
        r = lax.broadcasted_iota(jnp.int32, (size, size), 0)
        c = lax.broadcasted_iota(jnp.int32, (size, size), 1)
        tri = jnp.concatenate([(r >= c).astype(F32), (r <= c).astype(F32)], axis=0).astype(BF16)
        parts = thirds(ld)
        both = dot(tri, parts[0]) + (dot(tri, parts[1]) + dot(tri, parts[2]))
        lane = lax.broadcasted_iota(jnp.int32, (1, ld.shape[1]), 1)
        forward = lax.rem(lane, lanes2) < heads
        cum = jnp.where(forward, both[:size], both[size:])
        return cum, jnp.where(forward, cum[size - 1:size], cum[0:1])

    def conv(ref, taps, first, start, count, cols, size):
        outs = []
        for i in range(count):
            tc = slice(cols + i * 128, cols + (i + 1) * 128)
            v = (taps[0:1, tc] * ref[first + i, pl.ds(start + 7, size), :]
                 + taps[1:2, tc] * ref[first + i, pl.ds(start + 8, size), :]
                 + taps[2:3, tc] * ref[first + i, pl.ds(start + 9, size), :])
            outs.append(silu(v))
        return outs[0] if count == 1 else jnp.concatenate(outs, axis=1)

    gp, sig_first, rd_first = gw // 128, sw // 128, (inner + sw) // 128

    def widened(v, cols):
        return dot(widen(v), spread[:, cols])

    def span_states(sig_g, wr_g, w_f, w_b):
        rhs = jnp.concatenate([sig_g * w_f, sig_g * w_b], axis=1).astype(BF16)
        return lax.dot_general(wr_g, rhs, (((0,), (0,)), ((), ())), preferred_element_type=F32)

    def group_cols(side, g):
        return slice(side * inner + g * gw, side * inner + (g + 1) * gw)

    ctx_step = softplus(ctx_step_in + bias)
    ctx_cum, ctx_end = sums(rates * ctx_step, ctx_len)
    ctx_w = widen(jnp.exp(ctx_end - ctx_cum) * ctx_step)
    ctx_dec8 = widened(jnp.broadcast_to(jnp.exp(ctx_end), (8, lanes2)), slice(0, 2 * inner))
    ctx_dec[0] = ctx_dec8[:, :inner]
    ctx_dec[1] = ctx_dec8[:, inner:]
    for g in range(group_count):
        sig_g = conv(raw_c, sig_taps, sig_first + g * gp, 0, gp, g * gw, ctx_len)
        wr_g = conv(raw_c, wr_taps, g, 0, 1, g * STATE, ctx_len).astype(BF16)
        got = span_states(sig_g, wr_g, dot(ctx_w, spread[:, group_cols(0, g)]),
                          dot(ctx_w, spread[:, group_cols(1, g)]))
        ctx_acc[0, g] = got[:, :gw]
        ctx_acc[1, g] = got[:, gw:]

    def ctx_copy(side, g):
        dev = sp - 1 if side == 0 else sp + 1
        pairs = [(ctx_send.at[side, g], ctx_recv.at[side, g])]
        if g == 0:
            pairs.append((cdec_send.at[side], cdec_recv.at[side]))
        return [pltpu.make_async_remote_copy(
            src_ref=s, dst_ref=d, send_sem=cchain_sem.at[0, side, g, i],
            recv_sem=cchain_sem.at[1, side, g, i], device_id={"sp": dev}, device_id_type=MESH)
            for i, (s, d) in enumerate(pairs)]

    ctx_starts = (n - 1, 0)
    for side in range(2):
        @pl.when(sp == ctx_starts[side])
        def _():
            cdec_send[side] = ctx_dec[side]
            for g in range(group_count):
                ctx_send[side, g] = ctx_acc[side, g].astype(BF16)
                if n > 1:
                    for c in ctx_copy(side, g):
                        c.start()

    def ctx_hop(hop, g):
        if hop >= n or g >= group_count:
            return
        for side in range(2):
            @pl.when(sp == (n - 1 - hop if side == 0 else hop))
            def _():
                arrived(ctx_recv.at[side, g], cchain_sem.at[1, side, g, 0])
                if g == 0:
                    arrived(cdec_recv.at[side], cchain_sem.at[1, side, 0, 1])
                    if hop < n - 1:
                        cdec_send[side] = cdec_recv[side] * ctx_dec[side]
                ctx_acc[side, g] = (ctx_recv[side, g].astype(F32)
                                    + cdec_recv[side, 0:1, g * gw:(g + 1) * gw] * ctx_acc[side, g])
                if hop < n - 1:
                    ctx_send[side, g] = ctx_acc[side, g].astype(BF16)
                    for c in ctx_copy(side, g):
                        c.start()

    hidden_rows(lat_v, lat_rms, hid, 0, 0, length)
    ctx_hop(1, 0)
    st_raw = dot_t(hid[...], w_st[...]).astype(BF16).astype(F32)

    for g in range(1, group_count):
        ctx_hop(1, g)

    def by_block(v):
        return jnp.concatenate([v] * blocks, axis=1)

    step = softplus(jnp.concatenate([st_raw[b * BLOCK:(b + 1) * BLOCK] for b in range(blocks)], axis=1)
                    + by_block(bias))
    more = jnp.concatenate([extra[:, b * BLOCK:(b + 1) * BLOCK] for b in range(blocks)], axis=0).T
    cum, end = sums(by_block(rates) * step + more, BLOCK)
    weight, grow = jnp.exp(end - cum) * step, jnp.exp(cum)
    cum_t, step_t = cum.T, step.T
    ends = jnp.exp(end)
    for b in range(blocks):
        at_b = slice(b * lanes2, (b + 1) * lanes2)
        cum_col[b] = cum[:, at_b]
        ecum_col[b] = widen(grow[:, at_b])
        weight_col[b] = widen(weight[:, at_b])
        cum_row[b] = cum_t[at_b]
        step_row[b] = step_t[at_b]
        dec[b] = widened(jnp.broadcast_to(ends[:, at_b], (8, lanes2)), slice(0, 2 * inner))
    dec_all = dec[0]
    for b in range(1, blocks):
        dec_all = dec_all * dec[b]

    def project(first, size):
        got = dot(hid[...], w_all[:, first:first + size]).astype(BF16).astype(F32)
        for i in range(size // 128):
            raw[first // 128 + i, 8:8 + length, :] = got[:, i * 128:(i + 1) * 128]

    def gate_project():
        gates[...] = dot(hid[...], w_all[:, inner + 2 * sw:2 * inner + 2 * sw]).astype(BF16)

    def block_at(side, i):
        return i if side == 0 else blocks - 1 - i

    def side_cols(side):
        return slice(side * gw, (side + 1) * gw)

    def group_states(g):
        gc = slice(g * gw, (g + 1) * gw)

        def step(b, carry):
            start = pl.multiple_of(b * BLOCK, BLOCK)
            at = pl.ds(start, BLOCK)
            sig_g = conv(raw, sig_taps, sig_first + g * gp, start, gp, g * gw, BLOCK)
            wr_g = conv(raw, wr_taps, g, start, 1, g * STATE, BLOCK).astype(BF16)
            sig[at, gc] = sig_g.astype(BF16)
            wr[at, g * STATE:(g + 1) * STATE] = wr_g
            wide = weight_col[b]
            states[b, g] = span_states(sig_g, wr_g, dot(wide, spread[:, group_cols(0, g)]),
                                       dot(wide, spread[:, group_cols(1, g)]))
            return carry

        lax.fori_loop(0, blocks, step, 0, unroll=2)
        for side in range(2):
            def total_step(i, run):
                b = block_at(side, i)
                return run * dec[b, 0:1, group_cols(side, g)] + states[b, g, :, side_cols(side)]

            span_total[side, g] = lax.fori_loop(0, blocks, total_step, jnp.zeros((STATE, gw), F32))

    def chain_copy(side, g):
        dev = sp + 1 if side == 0 else sp - 1
        return pltpu.make_async_remote_copy(
            src_ref=chain_out.at[side, g], dst_ref=chain_in.at[side, g],
            send_sem=chain_sem.at[0, side, g], recv_sem=chain_sem.at[1, side, g],
            device_id={"sp": dev}, device_id_type=MESH)

    def chain_hop(hop, g):
        if hop < 0 or hop >= n:
            return
        for side in range(2):
            @pl.when(sp == (hop if side == 0 else n - 1 - hop))
            def _():
                if hop == 0:
                    chain_in[side, g] = ctx_acc[side, g].astype(BF16)
                else:
                    arrived(chain_in.at[side, g], chain_sem.at[1, side, g])
                if hop < n - 1:
                    chain_out[side, g] = (
                        chain_in[side, g].astype(F32) * dec_all[0:1, group_cols(side, g)]
                        + span_total[side, g]).astype(BF16)
                    chain_copy(side, g).start()

    def group_blocks(g):
        gc = slice(g * gw, (g + 1) * gw)

        def step(b, carry):
            start = pl.multiple_of(b * BLOCK, BLOCK)
            at = pl.ds(start, BLOCK)
            cr, sr, cc = cum_row[b], step_row[b], cum_col[b]
            lane_g = lax.broadcasted_iota(jnp.int32, (BLOCK, gw), 1)
            rd_g = conv(raw, rd_taps, rd_first + g, start, 1, g * STATE, BLOCK).astype(BF16)
            rd[at, g * STATE:(g + 1) * STATE] = rd_g
            wr_g = wr[at, g * STATE:(g + 1) * STATE]
            sig_g = sig[at, gc]
            pair = dot_t(rd_g, wr_g)
            mixes, sigs = [], []
            for e in range(per_group):
                f, k = g * per_group + e, heads + g * per_group + e
                gap = jnp.where(low_r >= low_c, cc[:, f:f + 1] - cr[f:f + 1], cc[:, k:k + 1] - cr[k:k + 1])
                sf, sk = sr[f:f + 1], sr[k:k + 1]
                size = jnp.where(low_r > low_c, sf, jnp.where(low_r < low_c, sk, sf + sk))
                mixes.append((jnp.exp(gap) * size * pair).astype(BF16))
                mine = (lane_g >= e * head_dim) & (lane_g < (e + 1) * head_dim)
                sigs.append(jnp.where(mine, sig_g, jnp.zeros_like(sig_g)))
            in_block[at, gc] = dot(jnp.concatenate(mixes, axis=1), jnp.concatenate(sigs, axis=0))
            return carry

        lax.fori_loop(0, blocks, step, 0, unroll=2)

    chunk = pl.ds(pl.multiple_of(place * gw, 128), gw)

    def norm_copy(g, b, cols, dev, slot, sender):
        ref = normed.at[g, pl.ds(pl.multiple_of(b * BLOCK, BLOCK), BLOCK), cols]
        return pltpu.make_async_remote_copy(
            src_ref=ref, dst_ref=ref, send_sem=norm_sem.at[0, slot, g, b],
            recv_sem=norm_sem.at[1, sender, g, b], device_id=dev, device_id_type=MESH)

    def place_cols(q):
        return pl.ds(pl.multiple_of(q * gw, 128), gw)

    def finish_group(g):
        gc = slice(g * gw, (g + 1) * gw)
        for side in range(2):
            def enter(i, run):
                b = block_at(side, i)
                ent[b, g, :, side_cols(side)] = run.astype(BF16)
                return run * dec[b, 0:1, group_cols(side, g)] + states[b, g, :, side_cols(side)]

            lax.fori_loop(0, blocks, enter, chain_in[side, g].astype(F32))

        def finish(b, carry):
            at = pl.ds(pl.multiple_of(b * BLOCK, BLOCK), BLOCK)
            carried = dot(rd[at, g * STATE:(g + 1) * STATE], ent[b, g])
            grown = ecum_col[b]
            both = (in_block[at, gc]
                    + carried[:, :gw] * dot(grown, spread[:, group_cols(0, g)])
                    + carried[:, gw:] * dot(grown, spread[:, group_cols(1, g)]))
            gated = both * silu(gates[at, gc].astype(F32))
            done = gated * inv_rms(gated) * group_gain[0:1, gc]
            normed[g, at, chunk] = done.astype(BF16)
            for k, a in enumerate(tp_peer):
                norm_copy(g, b, chunk, {"tp": a}, k, place).start()
            for k, p in enumerate(dp_peer):
                norm_copy(g, b, chunk, {"dp": p}, tps - 1 + k, place).start()
            return carry

        lax.fori_loop(0, blocks, finish, 0)

    ctx_hop(2, 0)
    project(0, sw + gw)
    for g in range(1, group_count):
        ctx_hop(2, g)
    group_states(0)
    for hop in range(3, n):
        ctx_hop(hop, 0)
    chain_hop(0, 0)
    project(sw + gw, inner + sw - gw)
    chain_hop(1, 0)
    for g in range(1, group_count):
        group_states(g)
        for hop in range(3, n):
            ctx_hop(hop, g)
        chain_hop(0, g)
    ld_gate.wait()
    group_blocks(0)
    chain_hop(2, 0)
    gate_project()
    for g in range(1, group_count):
        chain_hop(1, g)
    for g in range(group_count):
        if g > 0:
            group_blocks(g)
            chain_hop(2, g)
        for hop in range(3, n):
            chain_hop(hop, g)
        finish_group(g)

    for p in sp_peer:
        arrived(gate_in.at[p], mod_sem.at[3, p])
    gate_vec = gate_in[0]
    for q in range(1, n):
        gate_vec = gate_vec + gate_in[q]

    for c in ld_outs:
        c.wait()
    own_out = pl.ds(pl.multiple_of(place * out_cols, 128), out_cols)
    slots = (tps - 1) + (dps - 1)

    def relay(g, b):
        for k, a in enumerate(tp_peer):
            q = a * dps + dp
            norm_copy(g, b, place_cols(q), {"tp": a}, 0, q).wait_recv()
            for j, p in enumerate(dp_peer):
                slot = slots + k * (dps - 1) + j
                norm_copy(g, b, place_cols(q), {"dp": p}, slot, q).start()

    def gathered(g, b):
        for p in dp_peer:
            for a in range(tps):
                q = a * dps + p
                norm_copy(g, b, place_cols(q), {"dp": p}, 0, q).wait_recv()

    for g in range(group_count - 1):
        lax.fori_loop(0, blocks, lambda b, carry: (relay(g, b), carry)[1], 0)
        lax.fori_loop(0, blocks, lambda b, carry: (gathered(g, b), carry)[1], 0)
        part = dot(normed[g], w_o[g])
        acc[...] = part if g == 0 else acc[...] + part

    def finished(first, count):
        g = group_count - 1
        for b in range(first, first + count):
            gathered(g, b)
        at = pl.ds(first * BLOCK, count * BLOCK)
        part = dot(normed[g, at, :], w_o[g])
        if g > 0:
            part = part + acc[at, :]
        kept = lat_v[at, own_out].astype(F32)
        out[at, :] = (kept + gate_vec * part).astype(BF16)

    spans, first = [], 0
    while first < blocks:
        count = 2 if blocks - first > 2 else 1
        spans.append((first, count))
        first += count
    for i, (first, count) in enumerate(spans):
        for b in range(first, first + count):
            relay(group_count - 1, b)
        if i > 0:
            finished(*spans[i - 1])
    finished(*spans[-1])

    for c in sends:
        c.wait_send()

    @pl.when(sp < n - 1)
    def _():
        edge_copy(0).wait_send()

    @pl.when(sp > 0)
    def _():
        edge_copy(1).wait_send()

    for side in range(2):
        @pl.when(sp != ctx_starts[1 - side])
        def _():
            for g in range(group_count):
                for c in ctx_copy(side, g):
                    c.wait_send()

        @pl.when(sp != ctx_starts[side])
        def _():
            for g in range(group_count):
                chain_copy(side, g).wait_send()

    for g in range(group_count):
        def drained(b, carry):
            for k, a in enumerate(tp_peer):
                norm_copy(g, b, chunk, {"tp": a}, k, place).wait_send()
            for k, p in enumerate(dp_peer):
                norm_copy(g, b, chunk, {"dp": p}, tps - 1 + k, place).wait_send()
            for k, a in enumerate(tp_peer):
                for j, p in enumerate(dp_peer):
                    slot = slots + k * (dps - 1) + j
                    norm_copy(g, b, place_cols(a * dps + dp), {"dp": p}, slot, place).wait_send()
            return carry

        lax.fori_loop(0, blocks, drained, 0)


def on_device(dims, *args):
    (
        latent, context, condition, context_condition, shift_weight, scale_weight, gate_weight,
        norm_gain, out_gate_weight, signal_weight, writer_weight, reader_matrix, step_weight,
        signal_taps, writer_taps, reader_taps, step_bias, decay_log, decay_extra, group_gain,
        output_weight,
    ) = args
    n, tps, dps = dims
    half, width = latent.shape
    length = half * dps
    ctx_len = context.shape[0]
    heads = step_bias.shape[1]
    inner = signal_weight.shape[1]
    sw = writer_weight.shape[1]
    groups = sw // STATE
    gw = inner // groups
    blocks = length // BLOCK
    places = tps * dps
    mod_rows, mod_cols = shift_weight.shape
    out_cols = output_weight.shape[1]
    lanes2 = 2 * heads
    conv_cols = inner + 2 * sw
    steps = jnp.swapaxes(step_weight, 1, 2).reshape(lanes2, width)
    hbm = pl.BlockSpec(memory_space=pl.ANY)
    vmem = pl.BlockSpec(memory_space=pltpu.VMEM)
    slots = (tps - 1) + (dps - 1) + (tps - 1) * (dps - 1)
    peers = max(n - 1, places - 1, 1)
    scratch = [
        pltpu.VMEM((length, width), BF16),
        pltpu.VMEM((ctx_len, width), BF16),
        pltpu.VMEM((8, width), F32),
        pltpu.VMEM((3, mod_rows, mod_cols), BF16),
        pltpu.VMEM((4, mod_cols), F32),
        pltpu.VMEM((1, mod_cols), F32),
        pltpu.VMEM((n, 4, mod_cols), F32),
        pltpu.VMEM((n, 1, mod_cols), F32),
        pltpu.VMEM((4, mod_cols), F32),
        pltpu.VMEM((places, 4, mod_cols), F32),
        pltpu.VMEM((2, 8, width), F32),
        pltpu.VMEM((2, 8, width), F32),
        pltpu.VMEM((2, 2, width // 128, 128), F32),
        pltpu.VMEM((2, 2, width // 128, 128), F32),
        pltpu.VMEM((8, width), F32),
        pltpu.VMEM((length, width), BF16),
        pltpu.VMEM((ctx_len + 16, width), BF16),
        pltpu.VMEM((width, 2 * inner + 2 * sw), BF16),
        pltpu.VMEM((lanes2, width), BF16),
        pltpu.VMEM((groups, places * gw, out_cols), BF16),
        pltpu.VMEM((conv_cols // 128, length + 16, 128), F32),
        pltpu.VMEM((conv_cols // 128, ctx_len + 16, 128), F32),
        pltpu.VMEM((length, inner), BF16),
        pltpu.VMEM((length, 128), F32),
        pltpu.VMEM((ctx_len, 128), F32),
        pltpu.VMEM((blocks, BLOCK, lanes2), F32),
        pltpu.VMEM((blocks, BLOCK, 3 * lanes2), BF16),
        pltpu.VMEM((blocks, BLOCK, 3 * lanes2), BF16),
        pltpu.VMEM((blocks, lanes2, BLOCK), F32),
        pltpu.VMEM((blocks, lanes2, BLOCK), F32),
        pltpu.VMEM((length, inner), BF16),
        pltpu.VMEM((length, sw), BF16),
        pltpu.VMEM((length, sw), BF16),
        pltpu.VMEM((blocks, groups, STATE, 2 * gw), F32),
        pltpu.VMEM((blocks, 8, 2 * inner), F32),
        pltpu.VMEM((blocks, groups, STATE, 2 * gw), BF16),
        pltpu.VMEM((2, groups, STATE, gw), F32),
        pltpu.VMEM((2, 8, inner), F32),
        pltpu.VMEM((2, groups, STATE, gw), BF16),
        pltpu.VMEM((2, groups, STATE, gw), BF16),
        pltpu.VMEM((2, 8, inner), F32),
        pltpu.VMEM((2, 8, inner), F32),
        pltpu.VMEM((2, groups, STATE, gw), F32),
        pltpu.VMEM((2, groups, STATE, gw), BF16),
        pltpu.VMEM((2, groups, STATE, gw), BF16),
        pltpu.VMEM((3 * lanes2, 2 * inner), BF16),
        pltpu.VMEM((length, inner), F32),
        pltpu.VMEM((groups, length, places * gw), BF16),
        pltpu.VMEM((length, out_cols), F32),
        pltpu.SemaphoreType.DMA((10 + groups * places,)),
        pltpu.SemaphoreType.DMA((2, dps)),
        pltpu.SemaphoreType.DMA((6, max(n, places))),
        pltpu.SemaphoreType.DMA((2, 2)),
        pltpu.SemaphoreType.DMA((2, 2, groups, 2)),
        pltpu.SemaphoreType.DMA((2, 2, groups)),
        pltpu.SemaphoreType.DMA((2, max(slots, places), groups, blocks)),
    ]
    specs = [hbm, hbm, vmem, vmem, hbm, hbm, hbm, vmem, hbm, hbm, hbm, hbm, hbm,
             vmem, vmem, vmem, vmem, vmem, vmem, vmem, hbm]
    return pl.pallas_call(
        functools.partial(kernel, dims),
        out_shape=jax.ShapeDtypeStruct((length, out_cols), BF16),
        in_specs=specs,
        out_specs=vmem,
        scratch_shapes=scratch,
        compiler_params=pltpu.CompilerParams(
            collective_id=0, has_side_effects=True, vmem_limit_bytes=67043328),
    )(
        latent, context, condition, context_condition, shift_weight,
        scale_weight, gate_weight, norm_gain.reshape(1, -1), out_gate_weight, signal_weight,
        writer_weight, reader_matrix, steps, signal_taps, writer_taps, reader_taps, step_bias,
        decay_log, decay_extra.reshape(lanes2, length),
        group_gain.reshape(1, -1), output_weight,
    )


def solution(mesh):
    dims = (mesh.shape["sp"], mesh.shape["tp"], mesh.shape["dp"])
    in_specs = (
        P(("grp", "sp", "dp"), None),
        P(("grp", "sp"), None),
        P("grp"),
        P(),
        P("sp", ("tp", "dp")),
        P("sp", ("tp", "dp")),
        P("sp", ("tp", "dp")),
        P(),
        P(None, ("tp", "dp")),
        P(None, ("tp", "dp")),
        P(None, ("tp", "dp")),
        P(None, ("tp", "dp")),
        P(None, None, ("tp", "dp")),
        P(None, ("tp", "dp")),
        P(None, ("tp", "dp")),
        P(None, ("tp", "dp")),
        P(None, ("tp", "dp")),
        P(None, ("tp", "dp")),
        P(None, ("tp", "dp"), ("grp", "sp")),
        P(("tp", "dp")),
        P(None, ("tp", "dp")),
    )
    out_specs = P(("grp", "sp"), ("tp", "dp"))
    return jax.shard_map(
        functools.partial(on_device, dims), mesh=mesh, in_specs=in_specs, out_specs=out_specs,
        check_vma=False,
    )
```

time: 93.8 us -> 66.4 us (0.71)
  Pallas kernels: 81.6 us -> 63.5 us
  local copies, waits for them, and re-layouts: 10.4 us -> 2.67 us
  other arithmetic: 1.34 us -> 0 us
    pallas_call x1, Pallas kernels: 81.6 us -> 63.5 us  [on_device(): pl.pallas_call(functools.partial(kernel, dims), out_shape=jax.ShapeDtypeS...]
    reshape x4 -> x0, local copies, waits for them, and re-layouts: 5.19 us -> none  [the longest x1 1.35 us: on_device(): decay_log.reshape(1, lanes2)]
    concatenate x2 -> x0, other arithmetic: 1.34 us -> none  [the longest x1 1.33 us: on_device(): taps = jnp.concatenate([signal_taps, writer_taps, reader_taps], axis=1)]
    pad x1 -> x0, local copies, waits for them, and re-layouts: 1.18 us -> none  [on_device(): steps = jnp.pad(steps, ((0, 0), (0, 128 - lanes2)))]
where the time goes in v1:
time: 66.4 us; the launch traced here: 66.2 us
  Pallas kernels  63.5 us (96%)
  local copies, waits for them, and re-layouts  2.67 us (4%)
    pallas_call x1, Pallas kernels, on_device(): pl.pallas_call(functools.partial(kernel, dims), out_shape=jax.ShapeDtypeS...  63.5 us
    unnamed x1, local copies, waits for them, and re-layouts  2.67 us

profile of v1, /device:TPU:0, one launch (start us, length us, event | category | flops | bytes accessed | tf_op | source)
XLA Modules:
  0.0 66.2 jit_solution(4084498675352384024)
XLA Ops:
  0.0 63.5 %shard_map.199 = bf16[768,1024]{1,0:T(8,128)(2,1)} custom-call(bf16[384,4096]{1,0:T(8,128)(2,1)} %refs_0_.1, bf16[128,4096]{1,0:T(8,128)(2,1)} %refs_1_.1, bf16[4096]{0:T(1024)(128)(2,1)} %refs_2_.1, bf16[4096]{0:T(1024)(128)(2,1)} %refs_3_.1, bf16[1024,1024]{1,0:T(8,128)(2,1)} %refs_4_.1, bf16[1024,1024]{1,0:T(8,128)(2,1)} %refs_5_.1, ...), custom_call_target="tpu_custom_call" | custom-call | tf_op jit(solution)/shard_map/pallas_call | solution.py:756
  63.5 2.7 %copy.23 = bf16[768,1024]{1,0:T(8,128)(2,1)} copy(bf16[768,1024]{1,0:T(8,128)(2,1)} %shard_map.199) | data formatting | bytes 3145728

commit v2 on v1

--- a/solution.py
+++ b/solution.py
@@ -46,10 +46,10 @@
         w_gate, w_sig, w_wr, w_rd, w_step, sig_taps, wr_taps, rd_taps, step_bias, decay_log, extra,
         group_gain, w_out, out,
         lat_v, ctx_v, act, mod_w, mod_part, gate_part, mod_in, gate_in, mod_sum, mod_all,
-        scale_rows, shift_rows, edge_out, edge_in, edge_rows, hid, hid_c, w_all, w_st, w_o,
-        raw, raw_c, gates, lat_rms, ctx_rms, cum_col, ecum_col, weight_col, cum_row, step_row, sig, wr, rd,
-        states, dec, ent, ctx_acc, ctx_dec, ctx_send, ctx_recv, cdec_send, cdec_recv,
-        span_total, chain_out, chain_in, spread, in_block, normed, acc,
+        scale_rows, shift_rows, edge_out, edge_in, edge_rows, hid_c, w_all, w_st, w_o,
+        raw, raw_c, gates, cum_col, ecum_col, weight_col, cum_row, step_row, sig, wr, rd,
+        states, dec, ent, ctx_acc, ctx_send, ctx_recv, cdec_send, cdec_recv, sdec_send, sdec_recv,
+        span_total, chain_out, chain_recv, chain_in, spread, in_block, normed,
         load_sem, lat_sem, mod_sem, edge_sem, cchain_sem, chain_sem, norm_sem,
     ) = refs
     n, tps, dps = dims
@@ -81,18 +81,6 @@
 
     ld_shift = load(shift_w, mod_w.at[0])
     ld_scale = load(scale_w, mod_w.at[1])
-    ld_lat = load(latent, lat_v.at[pl.ds(dp * half, half)])
-    ld_ctx = load(context, ctx_v)
-    ld_gatew = load(gate_w, mod_w.at[2])
-    ld_sig = load(w_sig, w_all.at[:, pl.ds(sw, inner)])
-    ld_wr = load(w_wr, w_all.at[:, pl.ds(0, sw)])
-    ld_st = load(w_step, w_st)
-    ld_rd = load(w_rd, w_all.at[:, pl.ds(inner + sw, sw)])
-    ld_gate = load(w_gate, w_all.at[:, pl.ds(inner + 2 * sw, inner)])
-    ld_outs = [
-        load(w_out.at[pl.ds(q * inner + g * gw, gw)], w_o.at[g, pl.ds(q * gw, gw)])
-        for g in range(group_count) for q in range(places)
-    ]
 
     @pl.when(sp == 0)
     def _():
@@ -136,6 +124,18 @@
     mod_part[0:2, :] = dot(own_act, mod_w[0])[0:2]
     ld_scale.wait()
     mod_part[2:4, :] = dot(own_act, mod_w[1])[0:2]
+    ld_lat = load(latent, lat_v.at[pl.ds(dp * half, half)])
+    ld_ctx = load(context, ctx_v)
+    ld_gatew = load(gate_w, mod_w.at[0])
+    ld_sig = load(w_sig, w_all.at[:, pl.ds(sw, inner)])
+    ld_wr = load(w_wr, w_all.at[:, pl.ds(0, sw)])
+    ld_st = load(w_step, w_st)
+    ld_rd = load(w_rd, w_all.at[:, pl.ds(inner + sw, sw)])
+    ld_gate = load(w_gate, w_all.at[:, pl.ds(inner + 2 * sw, inner)])
+    ld_outs = [
+        load(w_out.at[pl.ds(q * inner + g * gw, gw)], w_o.at[g, pl.ds(q * gw, gw)])
+        for g in range(group_count) for q in range(places)
+    ]
     pl.semaphore_wait(barrier, len(sp_peer) + len(place_peer))
     for k, p in enumerate(sp_peer):
         sends.append(send(mod_part, mod_in.at[sp], mod_sem.at[0, k], mod_sem.at[1, sp], {"sp": p}))
@@ -147,6 +147,8 @@
 
     def inv_rms(v):
         return lax.rsqrt(jnp.mean(v * v, axis=-1, keepdims=True) + EPSILON)
+
+    lat_rms, ctx_rms = slice(0, 128), slice(128, 256)
 
     def row_tile(rows):
         return min(rows, 64)
@@ -161,7 +163,7 @@
                 v = ref[at, c * 128:(c + 1) * 128].astype(F32)
                 total = total + v * v
             mean = jnp.sum(total, axis=-1, keepdims=True) * (1.0 / width)
-            keep[at, :] = jnp.broadcast_to(lax.rsqrt(mean + EPSILON), (tile, 128))
+            in_block[at, keep] = jnp.broadcast_to(lax.rsqrt(mean + EPSILON), (tile, 128))
             return carry
 
         lax.fori_loop(0, count // tile, step, 0)
@@ -212,8 +214,16 @@
     for p in dp_peer:
         rms_rows(lat_v, lat_rms, p * half, half)
     rms_rows(ctx_v, ctx_rms, 0, ctx_len)
+    own_out = pl.ds(pl.multiple_of(place * out_cols, 128), out_cols)
+
+    def keep_rows(b, carry):
+        at = pl.ds(pl.multiple_of(b * BLOCK, BLOCK), BLOCK)
+        out[at, :] = lat_v[at, own_out]
+        return carry
+
+    lax.fori_loop(0, blocks, keep_rows, 0)
     ld_gatew.wait()
-    gate_part[...] = dot(own_act, mod_w[2])[0:1]
+    gate_part[...] = dot(own_act, mod_w[0])[0:1]
     for k, p in enumerate(sp_peer):
         sends.append(send(gate_part, gate_in.at[sp], mod_sem.at[2, k], mod_sem.at[3, sp], {"sp": p}))
     gate_in[sp] = gate_part[...]
@@ -244,7 +254,7 @@
 
         def step(t, carry):
             at = pl.ds(pl.multiple_of(start + t * tile, tile), tile)
-            r3 = keep[at, :].reshape(tile // 8, 8, 128)
+            r3 = in_block[at, keep].reshape(tile // 8, 8, 128)
             for c in range(width // 128):
                 cols = slice(c * 128, (c + 1) * 128)
                 v = ref[at, cols].astype(F32).reshape(tile // 8, 8, 128)
@@ -341,8 +351,6 @@
     ctx_cum, ctx_end = sums(rates * ctx_step, ctx_len)
     ctx_w = widen(jnp.exp(ctx_end - ctx_cum) * ctx_step)
     ctx_dec8 = widened(jnp.broadcast_to(jnp.exp(ctx_end), (8, lanes2)), slice(0, 2 * inner))
-    ctx_dec[0] = ctx_dec8[:, :inner]
-    ctx_dec[1] = ctx_dec8[:, inner:]
     for g in range(group_count):
         sig_g = conv(raw_c, sig_taps, sig_first + g * gp, 0, gp, g * gw, ctx_len)
         wr_g = conv(raw_c, wr_taps, g, 0, 1, g * STATE, ctx_len).astype(BF16)
@@ -351,51 +359,38 @@
         ctx_acc[0, g] = got[:, :gw]
         ctx_acc[1, g] = got[:, gw:]
 
-    def ctx_copy(side, g):
-        dev = sp - 1 if side == 0 else sp + 1
-        pairs = [(ctx_send.at[side, g], ctx_recv.at[side, g])]
-        if g == 0:
-            pairs.append((cdec_send.at[side], cdec_recv.at[side]))
-        return [pltpu.make_async_remote_copy(
-            src_ref=s, dst_ref=d, send_sem=cchain_sem.at[0, side, g, i],
-            recv_sem=cchain_sem.at[1, side, g, i], device_id={"sp": dev}, device_id_type=MESH)
-            for i, (s, d) in enumerate(pairs)]
-
-    ctx_starts = (n - 1, 0)
+    firsts = (0, n - 1)
+
+    def ctx_copy(side, part):
+        if part < group_count:
+            src, dst = ctx_send.at[side, part], ctx_recv.at[side, sp, part]
+        else:
+            src, dst = cdec_send.at[side], cdec_recv.at[side, sp]
+        return pltpu.make_async_remote_copy(
+            src_ref=src, dst_ref=dst, send_sem=cchain_sem.at[0, side, 0, part],
+            recv_sem=cchain_sem.at[1, side, sp, part], device_id={"sp": firsts[side]},
+            device_id_type=MESH)
+
     for side in range(2):
-        @pl.when(sp == ctx_starts[side])
-        def _():
-            cdec_send[side] = ctx_dec[side]
-            for g in range(group_count):
-                ctx_send[side, g] = ctx_acc[side, g].astype(BF16)
-                if n > 1:
-                    for c in ctx_copy(side, g):
-                        c.start()
-
-    def ctx_hop(hop, g):
-        if hop >= n or g >= group_count:
-            return
+        cdec_send[side] = ctx_dec8[0:1, side * inner:(side + 1) * inner]
+        ctx_send[side] = ctx_acc[side].astype(BF16)
+    for part in [group_count] + list(range(group_count)):
         for side in range(2):
-            @pl.when(sp == (n - 1 - hop if side == 0 else hop))
+            @pl.when(sp != firsts[side])
             def _():
-                arrived(ctx_recv.at[side, g], cchain_sem.at[1, side, g, 0])
-                if g == 0:
-                    arrived(cdec_recv.at[side], cchain_sem.at[1, side, 0, 1])
-                    if hop < n - 1:
-                        cdec_send[side] = cdec_recv[side] * ctx_dec[side]
-                ctx_acc[side, g] = (ctx_recv[side, g].astype(F32)
-                                    + cdec_recv[side, 0:1, g * gw:(g + 1) * gw] * ctx_acc[side, g])
-                if hop < n - 1:
-                    ctx_send[side, g] = ctx_acc[side, g].astype(BF16)
-                    for c in ctx_copy(side, g):
-                        c.start()
-
-    hidden_rows(lat_v, lat_rms, hid, 0, 0, length)
-    ctx_hop(1, 0)
-    st_raw = dot_t(hid[...], w_st[...]).astype(BF16).astype(F32)
-
-    for g in range(1, group_count):
-        ctx_hop(1, g)
+                ctx_copy(side, part).start()
+
+    def ctx_collect(side, g):
+        for d in range(1, n):
+            q = d if side == 0 else n - 1 - d
+            if g == 0:
+                arrived(cdec_recv.at[side, q], cchain_sem.at[1, side, q, group_count])
+            arrived(ctx_recv.at[side, q, g], cchain_sem.at[1, side, q, g])
+            ctx_acc[side, g] = (ctx_acc[side, g] * cdec_recv[side, q, :, g * gw:(g + 1) * gw]
+                                + ctx_recv[side, q, g].astype(F32))
+
+    hidden_rows(lat_v, lat_rms, lat_v, 0, 0, length)
+    st_raw = dot_t(lat_v[...], w_st[...]).astype(BF16).astype(F32)
 
     def by_block(v):
         return jnp.concatenate([v] * blocks, axis=1)
@@ -418,14 +413,86 @@
     dec_all = dec[0]
     for b in range(1, blocks):
         dec_all = dec_all * dec[b]
+    for side in range(2):
+        sdec_send[side] = dec_all[0:1, side * inner:(side + 1) * inner]
+
+    def chain_copy(side, d, part):
+        if part < group_count:
+            src, dst = chain_out.at[side, part], chain_recv.at[side, sp, part]
+        else:
+            src, dst = sdec_send.at[side], sdec_recv.at[side, sp]
+        return pltpu.make_async_remote_copy(
+            src_ref=src, dst_ref=dst, send_sem=chain_sem.at[0, side, d, part],
+            recv_sem=chain_sem.at[1, side, sp, part],
+            device_id={"sp": sp + d if side == 0 else sp - d}, device_id_type=MESH)
+
+    def has_goal(side, d):
+        return sp + d < n if side == 0 else sp - d >= 0
+
+    def is_source(side, q):
+        return sp > q if side == 0 else sp < q
+
+    for d in range(n - 1, 0, -1):
+        for side in range(2):
+            @pl.when(has_goal(side, d) & (sp != firsts[side]))
+            def _():
+                chain_copy(side, d, group_count).start()
+
+    def chain_start(g):
+        for side in range(2):
+            @pl.when(sp == firsts[side])
+            def _():
+                ctx_collect(side, g)
+                if n > 1:
+                    chain_out[side, g] = (ctx_acc[side, g] * dec_all[0:1, group_cols(side, g)]
+                                          + span_total[side, g]).astype(BF16)
+
+            @pl.when(sp != firsts[side])
+            def _():
+                chain_out[side, g] = span_total[side, g].astype(BF16)
+        for d in range(n - 1, 0, -1):
+            for side in range(2):
+                @pl.when(has_goal(side, d))
+                def _():
+                    chain_copy(side, d, g).start()
+
+    def chain_end(g):
+        for side in range(2):
+            @pl.when(sp == firsts[side])
+            def _():
+                chain_in[side, g] = ctx_acc[side, g]
+
+            if n > 1:
+                @pl.when(sp != firsts[side])
+                def _():
+                    arrived(chain_recv.at[side, firsts[side], g], chain_sem.at[1, side, firsts[side], g])
+                    chain_in[side, g] = chain_recv[side, firsts[side], g].astype(F32)
+
+            for d in range(1, n - 1):
+                q = d if side == 0 else n - 1 - d
+
+                @pl.when(is_source(side, q))
+                def _():
+                    if g == 0:
+                        arrived(sdec_recv.at[side, q], chain_sem.at[1, side, q, group_count])
+                    arrived(chain_recv.at[side, q, g], chain_sem.at[1, side, q, g])
+                    chain_in[side, g] = (
+                        chain_in[side, g] * sdec_recv[side, q, :, g * gw:(g + 1) * gw]
+                        + chain_recv[side, q, g].astype(F32))
+
+    def hidden_dot(first, size):
+        if size % 512 == 0:
+            return dot(lat_v[...], w_all[:, first:first + size])
+        near = dot(lat_v[:, :width // 2], w_all[:width // 2, first:first + size])
+        return near + dot(lat_v[:, width // 2:], w_all[width // 2:, first:first + size])
 
     def project(first, size):
-        got = dot(hid[...], w_all[:, first:first + size]).astype(BF16).astype(F32)
+        got = hidden_dot(first, size).astype(BF16).astype(F32)
         for i in range(size // 128):
             raw[first // 128 + i, 8:8 + length, :] = got[:, i * 128:(i + 1) * 128]
 
-    def gate_project():
-        gates[...] = dot(hid[...], w_all[:, inner + 2 * sw:2 * inner + 2 * sw]).astype(BF16)
+    def gate_project(g):
+        gates[:, g * gw:(g + 1) * gw] = hidden_dot(inner + 2 * sw + g * gw, gw).astype(BF16)
 
     def block_at(side, i):
         return i if side == 0 else blocks - 1 - i
@@ -455,29 +522,6 @@
                 return run * dec[b, 0:1, group_cols(side, g)] + states[b, g, :, side_cols(side)]
 
             span_total[side, g] = lax.fori_loop(0, blocks, total_step, jnp.zeros((STATE, gw), F32))
-
-    def chain_copy(side, g):
-        dev = sp + 1 if side == 0 else sp - 1
-        return pltpu.make_async_remote_copy(
-            src_ref=chain_out.at[side, g], dst_ref=chain_in.at[side, g],
-            send_sem=chain_sem.at[0, side, g], recv_sem=chain_sem.at[1, side, g],
-            device_id={"sp": dev}, device_id_type=MESH)
-
-    def chain_hop(hop, g):
-        if hop < 0 or hop >= n:
-            return
-        for side in range(2):
-            @pl.when(sp == (hop if side == 0 else n - 1 - hop))
-            def _():
-                if hop == 0:
-                    chain_in[side, g] = ctx_acc[side, g].astype(BF16)
-                else:
-                    arrived(chain_in.at[side, g], chain_sem.at[1, side, g])
-                if hop < n - 1:
-                    chain_out[side, g] = (
-                        chain_in[side, g].astype(F32) * dec_all[0:1, group_cols(side, g)]
-                        + span_total[side, g]).astype(BF16)
-                    chain_copy(side, g).start()
 
     def group_blocks(g):
         gc = slice(g * gw, (g + 1) * gw)
@@ -525,7 +569,7 @@
                 ent[b, g, :, side_cols(side)] = run.astype(BF16)
                 return run * dec[b, 0:1, group_cols(side, g)] + states[b, g, :, side_cols(side)]
 
-            lax.fori_loop(0, blocks, enter, chain_in[side, g].astype(F32))
+            lax.fori_loop(0, blocks, enter, chain_in[side, g])
 
         def finish(b, carry):
             at = pl.ds(pl.multiple_of(b * BLOCK, BLOCK), BLOCK)
@@ -545,33 +589,20 @@
 
         lax.fori_loop(0, blocks, finish, 0)
 
-    ctx_hop(2, 0)
     project(0, sw + gw)
+    group_states(0)
+    chain_start(0)
     for g in range(1, group_count):
-        ctx_hop(2, g)
-    group_states(0)
-    for hop in range(3, n):
-        ctx_hop(hop, 0)
-    chain_hop(0, 0)
-    project(sw + gw, inner + sw - gw)
-    chain_hop(1, 0)
+        project(sw + g * gw, gw)
+        group_states(g)
+    project(sw + inner, sw)
     for g in range(1, group_count):
-        group_states(g)
-        for hop in range(3, n):
-            ctx_hop(hop, g)
-        chain_hop(0, g)
+        chain_start(g)
     ld_gate.wait()
-    group_blocks(0)
-    chain_hop(2, 0)
-    gate_project()
-    for g in range(1, group_count):
-        chain_hop(1, g)
     for g in range(group_count):
-        if g > 0:
-            group_blocks(g)
-            chain_hop(2, g)
-        for hop in range(3, n):
-            chain_hop(hop, g)
+        group_blocks(g)
+        gate_project(g)
+        chain_end(g)
         finish_group(g)
 
     for p in sp_peer:
@@ -582,7 +613,6 @@
 
     for c in ld_outs:
         c.wait()
-    own_out = pl.ds(pl.multiple_of(place * out_cols, 128), out_cols)
     slots = (tps - 1) + (dps - 1)
 
     def relay(g, b):
@@ -599,11 +629,19 @@
                 q = a * dps + p
                 norm_copy(g, b, place_cols(q), {"dp": p}, 0, q).wait_recv()
 
+    def held(b):
+        return jnp.concatenate([states[b, j] for j in range(group_count)], axis=1)
+
     for g in range(group_count - 1):
         lax.fori_loop(0, blocks, lambda b, carry: (relay(g, b), carry)[1], 0)
         lax.fori_loop(0, blocks, lambda b, carry: (gathered(g, b), carry)[1], 0)
         part = dot(normed[g], w_o[g])
-        acc[...] = part if g == 0 else acc[...] + part
+        for b in range(blocks):
+            piece = part[b * BLOCK:(b + 1) * BLOCK]
+            if g > 0:
+                piece = piece + held(b)
+            for j in range(group_count):
+                states[b, j] = piece[:, j * 2 * gw:(j + 1) * 2 * gw]
 
     def finished(first, count):
         g = group_count - 1
@@ -612,9 +650,8 @@
         at = pl.ds(first * BLOCK, count * BLOCK)
         part = dot(normed[g, at, :], w_o[g])
         if g > 0:
-            part = part + acc[at, :]
-        kept = lat_v[at, own_out].astype(F32)
-        out[at, :] = (kept + gate_vec * part).astype(BF16)
+            part = part + jnp.concatenate([held(b) for b in range(first, first + count)], axis=0)
+        out[at, :] = (out[at, :].astype(F32) + gate_vec * part).astype(BF16)
 
     spans, first = [], 0
     while first < blocks:
@@ -640,16 +677,20 @@
         edge_copy(1).wait_send()
 
     for side in range(2):
-        @pl.when(sp != ctx_starts[1 - side])
+        @pl.when(sp != firsts[side])
         def _():
-            for g in range(group_count):
-                for c in ctx_copy(side, g):
-                    c.wait_send()
-
-        @pl.when(sp != ctx_starts[side])
-        def _():
-            for g in range(group_count):
-                chain_copy(side, g).wait_send()
+            for part in range(group_count + 1):
+                ctx_copy(side, part).wait_send()
+
+        for d in range(1, n):
+            @pl.when(has_goal(side, d))
+            def _():
+                for g in range(group_count):
+                    chain_copy(side, d, g).wait_send()
+
+            @pl.when(has_goal(side, d) & (sp != firsts[side]))
+            def _():
+                chain_copy(side, d, group_count).wait_send()
 
     for g in range(group_count):
         def drained(b, carry):
@@ -689,7 +730,7 @@
     lanes2 = 2 * heads
     conv_cols = inner + 2 * sw
     steps = jnp.swapaxes(step_weight, 1, 2).reshape(lanes2, width)
-    hbm = pl.BlockSpec(memory_space=pl.ANY)
+    hbm = pl.BlockSpec(memory_space=pltpu.HBM)
     vmem = pl.BlockSpec(memory_space=pltpu.VMEM)
     slots = (tps - 1) + (dps - 1) + (tps - 1) * (dps - 1)
     peers = max(n - 1, places - 1, 1)
@@ -697,7 +738,7 @@
         pltpu.VMEM((length, width), BF16),
         pltpu.VMEM((ctx_len, width), BF16),
         pltpu.VMEM((8, width), F32),
-        pltpu.VMEM((3, mod_rows, mod_cols), BF16),
+        pltpu.VMEM((2, mod_rows, mod_cols), BF16),
         pltpu.VMEM((4, mod_cols), F32),
         pltpu.VMEM((1, mod_cols), F32),
         pltpu.VMEM((n, 4, mod_cols), F32),
@@ -709,7 +750,6 @@
         pltpu.VMEM((2, 2, width // 128, 128), F32),
         pltpu.VMEM((2, 2, width // 128, 128), F32),
         pltpu.VMEM((8, width), F32),
-        pltpu.VMEM((length, width), BF16),
         pltpu.VMEM((ctx_len + 16, width), BF16),
         pltpu.VMEM((width, 2 * inner + 2 * sw), BF16),
         pltpu.VMEM((lanes2, width), BF16),
@@ -717,8 +757,6 @@
         pltpu.VMEM((conv_cols // 128, length + 16, 128), F32),
         pltpu.VMEM((conv_cols // 128, ctx_len + 16, 128), F32),
         pltpu.VMEM((length, inner), BF16),
-        pltpu.VMEM((length, 128), F32),
-        pltpu.VMEM((ctx_len, 128), F32),
         pltpu.VMEM((blocks, BLOCK, lanes2), F32),
         pltpu.VMEM((blocks, BLOCK, 3 * lanes2), BF16),
         pltpu.VMEM((blocks, BLOCK, 3 * lanes2), BF16),
@@ -731,43 +769,44 @@
         pltpu.VMEM((blocks, 8, 2 * inner), F32),
         pltpu.VMEM((blocks, groups, STATE, 2 * gw), BF16),
         pltpu.VMEM((2, groups, STATE, gw), F32),
-        pltpu.VMEM((2, 8, inner), F32),
         pltpu.VMEM((2, groups, STATE, gw), BF16),
-        pltpu.VMEM((2, groups, STATE, gw), BF16),
-        pltpu.VMEM((2, 8, inner), F32),
-        pltpu.VMEM((2, 8, inner), F32),
+        pltpu.VMEM((2, n, groups, STATE, gw), BF16),
+        pltpu.VMEM((2, 1, inner), F32),
+        pltpu.VMEM((2, n, 1, inner), F32),
+        pltpu.VMEM((2, 1, inner), F32),
+        pltpu.VMEM((2, n, 1, inner), F32),
         pltpu.VMEM((2, groups, STATE, gw), F32),
         pltpu.VMEM((2, groups, STATE, gw), BF16),
-        pltpu.VMEM((2, groups, STATE, gw), BF16),
+        pltpu.VMEM((2, n, groups, STATE, gw), BF16),
+        pltpu.VMEM((2, groups, STATE, gw), F32),
         pltpu.VMEM((3 * lanes2, 2 * inner), BF16),
         pltpu.VMEM((length, inner), F32),
         pltpu.VMEM((groups, length, places * gw), BF16),
-        pltpu.VMEM((length, out_cols), F32),
         pltpu.SemaphoreType.DMA((10 + groups * places,)),
         pltpu.SemaphoreType.DMA((2, dps)),
         pltpu.SemaphoreType.DMA((6, max(n, places))),
         pltpu.SemaphoreType.DMA((2, 2)),
-        pltpu.SemaphoreType.DMA((2, 2, groups, 2)),
-        pltpu.SemaphoreType.DMA((2, 2, groups)),
+        pltpu.SemaphoreType.DMA((2, 2, n, groups + 1)),
+        pltpu.SemaphoreType.DMA((2, 2, n, groups + 1)),
         pltpu.SemaphoreType.DMA((2, max(slots, places), groups, blocks)),
     ]
     specs = [hbm, hbm, vmem, vmem, hbm, hbm, hbm, vmem, hbm, hbm, hbm, hbm, hbm,
              vmem, vmem, vmem, vmem, vmem, vmem, vmem, hbm]
+    operands = (
+        latent, context, condition, context_condition, shift_weight, scale_weight, gate_weight,
+        norm_gain.reshape(1, -1), out_gate_weight, signal_weight, writer_weight, reader_matrix,
+        steps, signal_taps, writer_taps, reader_taps, step_bias, decay_log,
+        decay_extra.reshape(lanes2, length), group_gain.reshape(1, -1), output_weight,
+    )
     return pl.pallas_call(
         functools.partial(kernel, dims),
-        out_shape=jax.ShapeDtypeStruct((length, out_cols), BF16),
+        out_shape=pltpu.VMEM((length, out_cols), BF16),
         in_specs=specs,
         out_specs=vmem,
         scratch_shapes=scratch,
         compiler_params=pltpu.CompilerParams(
-            collective_id=0, has_side_effects=True, vmem_limit_bytes=67043328),
-    )(
-        latent, context, condition, context_condition, shift_weight,
-        scale_weight, gate_weight, norm_gain.reshape(1, -1), out_gate_weight, signal_weight,
-        writer_weight, reader_matrix, steps, signal_taps, writer_taps, reader_taps, step_bias,
-        decay_log, decay_extra.reshape(lanes2, length),
-        group_gain.reshape(1, -1), output_weight,
-    )
+            collective_id=0, has_side_effects=True, vmem_limit_bytes=60000000),
+    )(*[pltpu.with_memory_space_constraint(x, pltpu.HBM) for x in operands])
 
 
 def solution(mesh):

time: 66.4 us -> 62.1 us (0.935)
  Pallas kernels: 63.5 us -> 60.4 us
  local copies, waits for them, and re-layouts: 2.67 us -> 1.15 us
    pallas_call x1, Pallas kernels: 63.5 us -> 60.4 us  [on_device(): pl.pallas_call(functools.partial(kernel, dims), out_shape=pltpu.VMEM((len...]
    unnamed x1, local copies, waits for them, and re-layouts: 2.67 us -> 1.15 us
where the time goes in v2:
time: 62.1 us; the launch traced here: 61.6 us
  Pallas kernels  60.4 us (97%)
  local copies, waits for them, and re-layouts  1.15 us (2%)
    pallas_call x1, Pallas kernels, on_device(): pl.pallas_call(functools.partial(kernel, dims), out_shape=pltpu.VMEM((len...  60.4 us

profile of v2, /device:TPU:0, one launch (start us, length us, event | category | flops | bytes accessed | tf_op | source)
XLA Modules:
  0.0 61.6 jit_solution(9099872146879895684)
XLA Ops:
  0.0 60.4 %shard_map.199 = bf16[768,1024]{1,0:T(8,128)(2,1)S(1)} custom-call(bf16[384,4096]{1,0:T(8,128)(2,1)} %refs_0_.1, bf16[128,4096]{1,0:T(8,128)(2,1)} %refs_1_.1, bf16[4096]{0:T(1024)(128)(2,1)} %refs_2_.1, bf16[4096]{0:T(1024)(128)(2,1)} %refs_3_.1, bf16[1024,1024]{1,0:T(8,128)(2,1)} %refs_4_.1, bf16[1024,1024]{1,0:T(8,128)(2,1)} %refs_5_.1, ...), custom_call_target="tpu_custom_call" | custom-call | tf_op jit(solution)/shard_map/pallas_call | solution.py:801
  60.5 1.1 %copy.23 = bf16[768,1024]{1,0:T(8,128)(2,1)} copy(bf16[768,1024]{1,0:T(8,128)(2,1)S(1)} %shard_map.199) | data formatting | bytes 3145728

commit v3 on v2

--- a/solution.py
+++ b/solution.py
@@ -42,9 +42,10 @@
 
 def kernel(dims, *refs):
     (
-        latent, context, cond, ctx_cond, shift_w, scale_w, gate_w, gain,
-        w_gate, w_sig, w_wr, w_rd, w_step, sig_taps, wr_taps, rd_taps, step_bias, decay_log, extra,
-        group_gain, w_out, out,
+        latent, context, cond_h, ctx_cond_h, shift_w, scale_w, gate_w, gain_h,
+        w_gate, w_sig, w_wr, w_rd, w_step, sig_taps_h, wr_taps_h, rd_taps_h, step_bias_h, decay_log_h,
+        extra_h, group_gain_h, w_out, out,
+        cond, ctx_cond, gain, sig_taps, wr_taps, rd_taps, step_bias, decay_log, extra, group_gain,
         lat_v, ctx_v, act, mod_w, mod_part, gate_part, mod_in, gate_in, mod_sum, mod_all,
         scale_rows, shift_rows, edge_out, edge_in, edge_rows, hid_c, w_all, w_st, w_o,
         raw, raw_c, gates, cum_col, ecum_col, weight_col, cum_row, step_row, sig, wr, rd,
@@ -79,6 +80,7 @@
         loads.append(c)
         return c
 
+    ld_conds = [load(cond_h, cond), load(ctx_cond_h, ctx_cond)]
     ld_shift = load(shift_w, mod_w.at[0])
     ld_scale = load(scale_w, mod_w.at[1])
 
@@ -116,6 +118,8 @@
     def arrived(dst, rsem):
         pltpu.make_async_copy(dst, dst, rsem).wait()
 
+    for c in ld_conds:
+        c.wait()
     act[...] = jnp.zeros(act.shape, F32)
     act[0:1, :] = silu(cond[...].astype(F32)).astype(BF16).astype(F32).reshape(1, -1)
     act[1:2, :] = silu(ctx_cond[...].astype(F32)).astype(BF16).astype(F32).reshape(1, -1)
@@ -124,6 +128,9 @@
     mod_part[0:2, :] = dot(own_act, mod_w[0])[0:2]
     ld_scale.wait()
     mod_part[2:4, :] = dot(own_act, mod_w[1])[0:2]
+    ld_small = [load(src, dst) for src, dst in (
+        (gain_h, gain), (sig_taps_h, sig_taps), (wr_taps_h, wr_taps), (rd_taps_h, rd_taps),
+        (step_bias_h, step_bias), (decay_log_h, decay_log), (extra_h, extra), (group_gain_h, group_gain))]
     ld_lat = load(latent, lat_v.at[pl.ds(dp * half, half)])
     ld_ctx = load(context, ctx_v)
     ld_gatew = load(gate_w, mod_w.at[0])
@@ -239,6 +246,8 @@
     def widen(v):
         return jnp.concatenate(thirds(v), axis=1)
 
+    for c in ld_small:
+        c.wait()
     for a, b in place_peer:
         arrived(mod_all.at[a * dps + b], mod_sem.at[5, a * dps + b])
     for j in range(places):
@@ -734,7 +743,10 @@
     vmem = pl.BlockSpec(memory_space=pltpu.VMEM)
     slots = (tps - 1) + (dps - 1) + (tps - 1) * (dps - 1)
     peers = max(n - 1, places - 1, 1)
-    scratch = [
+    small = (condition, context_condition, norm_gain.reshape(1, -1), signal_taps, writer_taps,
+             reader_taps, step_bias, decay_log, decay_extra.reshape(lanes2, length),
+             group_gain.reshape(1, -1))
+    scratch = [pltpu.VMEM(v.shape, v.dtype) for v in small] + [
         pltpu.VMEM((length, width), BF16),
         pltpu.VMEM((ctx_len, width), BF16),
         pltpu.VMEM((8, width), F32),
@@ -782,7 +794,7 @@
         pltpu.VMEM((3 * lanes2, 2 * inner), BF16),
         pltpu.VMEM((length, inner), F32),
         pltpu.VMEM((groups, length, places * gw), BF16),
-        pltpu.SemaphoreType.DMA((10 + groups * places,)),
+        pltpu.SemaphoreType.DMA((20 + groups * places,)),
         pltpu.SemaphoreType.DMA((2, dps)),
         pltpu.SemaphoreType.DMA((6, max(n, places))),
         pltpu.SemaphoreType.DMA((2, 2)),
@@ -790,8 +802,7 @@
         pltpu.SemaphoreType.DMA((2, 2, n, groups + 1)),
         pltpu.SemaphoreType.DMA((2, max(slots, places), groups, blocks)),
     ]
-    specs = [hbm, hbm, vmem, vmem, hbm, hbm, hbm, vmem, hbm, hbm, hbm, hbm, hbm,
-             vmem, vmem, vmem, vmem, vmem, vmem, vmem, hbm]
+    specs = [hbm] * 21
     operands = (
         latent, context, condition, context_condition, shift_weight, scale_weight, gate_weight,
         norm_gain.reshape(1, -1), out_gate_weight, signal_weight, writer_weight, reader_matrix,

time: 62.1 us -> 61.2 us (0.986)
  Pallas kernels: 60.4 us -> 59.6 us
    pallas_call x1, Pallas kernels: 60.4 us -> 59.6 us  [on_device(): pl.pallas_call(functools.partial(kernel, dims), out_shape=pltpu.VMEM((len...]
where the time goes in v3:
time: 61.2 us; the launch traced here: 60.8 us
  Pallas kernels  59.6 us (97%)
  local copies, waits for them, and re-layouts  1.15 us (2%)
    pallas_call x1, Pallas kernels, on_device(): pl.pallas_call(functools.partial(kernel, dims), out_shape=pltpu.VMEM((len...  59.6 us

profile of v3, /device:TPU:0, one launch (start us, length us, event | category | flops | bytes accessed | tf_op | source)
XLA Modules:
  0.0 60.8 jit_solution(17202906694611172243)
XLA Ops:
  0.0 59.6 %shard_map.199 = bf16[768,1024]{1,0:T(8,128)(2,1)S(1)} custom-call(bf16[384,4096]{1,0:T(8,128)(2,1)} %refs_0_.1, bf16[128,4096]{1,0:T(8,128)(2,1)} %refs_1_.1, bf16[4096]{0:T(1024)(128)(2,1)} %refs_2_.1, bf16[4096]{0:T(1024)(128)(2,1)} %refs_3_.1, bf16[1024,1024]{1,0:T(8,128)(2,1)} %refs_4_.1, bf16[1024,1024]{1,0:T(8,128)(2,1)} %refs_5_.1, ...), custom_call_target="tpu_custom_call" | custom-call | tf_op jit(solution)/shard_map/pallas_call | solution.py:812
  59.6 1.1 %copy.23 = bf16[768,1024]{1,0:T(8,128)(2,1)} copy(bf16[768,1024]{1,0:T(8,128)(2,1)S(1)} %shard_map.199) | data formatting | bytes 3145728
